TPU v7x, 256 devices: a 4x2x16 block of a 4x16x16 slice. The times are simulated.
256 devices in a mesh: grp: 2 (over y), fs: 16 (over z), tp: 8 (over x, core).
Axes of the slice: x: 4, y: 2, z: 16, core: 2. Of those that a mesh axis runs over, the one named last changes fastest.
The devices are a block of a 4x16x16 slice.
Arguments:
- block_source_tensor: bfloat16 [16384, 2048], P(('grp', 'fs'), 'tp'), parts along dimension 0, may hold values from -6 to 6
- attend_initial_norm_gain: float32 [2048], replicated, may hold values from 0.1 to 1.9
- each_channel_group_norm: float32 [8, 256], P('tp'), may hold values from 0.1 to 1.9
- attend_final_norm_gain: float32 [2048], replicated, may hold values from 0.1 to 1.9
- dense_initial_norm_gain: float32 [2048], replicated, may hold values from 0.1 to 1.9
- dense_final_norm_gain: float32 [2048], replicated, may hold values from 0.1 to 1.9
- question_map: bfloat16 [2048, 1024], P('fs', 'tp'), may hold values from -0.125 to 0.125
- address_map: bfloat16 [2048, 1024], P('fs', 'tp'), may hold values from -0.125 to 0.125
- payload_weights_map: bfloat16 [2048, 2048], P('fs', 'tp'), may hold values from -0.125 to 0.125
- fading_left_factor: bfloat16 [2048, 16], replicated, may hold values from -0.125 to 0.125
- fading_right_factor: float32 [16, 1024], P(None, 'tp'), may hold values from -1.5 to 1.5
- fading_valve_constant: float32 [1024], P('tp'), may hold values from 0.05 to 6.2
- sudden_fade_excess: float32 [16384, 1024], P(('grp', 'fs'), 'tp'), parts along dimension 0, may hold values from -0.7 to 0
- combining_map: bfloat16 [2048, 2048], P('tp', 'fs')
- valve_map: bfloat16 [2048, 3072], P('fs', 'tp'), may hold values from -0.125 to 0.125
- widening_map: bfloat16 [2048, 3072], P('fs', 'tp'), may hold values from -0.125 to 0.125
- valve_conv_stencil: bfloat16 [3, 3072], P(None, 'tp'), may hold values from -3.5 to 3.5
- widening_conv_stencil: bfloat16 [3, 3072], P(None, 'tp'), may hold values from -3.5 to 3.5
- narrowing_map: bfloat16 [3072, 2048], P('tp', 'fs')
Outputs:
- layer_out: bfloat16 [16384, 2048], P(('grp', 'fs'), 'tp'), parts along dimension 0
There are 2 independent parts, one for each index of `grp`. A program takes and returns all parts, laid end to end along the dimension named above; an argument that names none is the same for every part. Nothing has to cross between parts.
All inputs are finite; a program needn't handle non-finite values.
Results may differ from a plain program's by a relative error of at most 0.019.
Values may be sent and summed in bfloat16 or wider, within the bound.
A program may use at most 64 MiB of HBM per device.

v0:
```python
import jax
import jax.numpy as jnp
from jax import lax
from jax.sharding import PartitionSpec as P

KEY_DIM = 128
VALUE_DIM = 256
BLOCK = 16


epsilon = 1e-06
valve_steepness = 16.0
careful_evaluation = lax.Precision.HIGHEST


def copy_for_each(value, axis):
    copies = jnp.broadcast_to(value, (lax.axis_size(axis), *value.shape))
    return lax.all_to_all(copies, axis, split_axis=0, concat_axis=0, tiled=True)


def laid_out(tiles, dim):
    lengths = list(tiles.shape[1:])
    lengths[dim] *= tiles.shape[0]
    return jnp.moveaxis(tiles, 0, dim).reshape(lengths)


def gathered_copies(value, axis, dim):
    tiles = copy_for_each(value, axis)
    return laid_out(tiles, dim)


def in_one_piece(arrays, axis, dim, along):
    ends, at = ([], 0)
    for a in arrays[:-1]:
        at += a.shape[along]
        ends.append(at)
    both = jnp.concatenate(arrays, axis=along)
    return tuple(jnp.split(lax.all_gather(both, axis, axis=dim, tiled=True), ends, axis=along))


def in_blocks(value, dim, count):
    before, after = (value.shape[:dim], value.shape[dim + 1 :])
    return jnp.moveaxis(value.reshape(*before, count, -1, *after), dim, 0)


def sum_at_owner(value, axis, dim):
    tiles = in_blocks(value, dim, lax.axis_size(axis))
    arrived = lax.all_to_all(tiles, axis, split_axis=0, concat_axis=0, tiled=True)
    return arrived.astype(jnp.float32).sum(axis=0)


def of_everyone(value, axis):
    everything = copy_for_each(value, axis)
    return jnp.sum(everything, axis=0)


def norm_rows(values, channel_gain):
    return (
        values
        * lax.rsqrt(jnp.mean(values * values, axis=-1, keepdims=True) + epsilon)
        * channel_gain
    )


def rounded(values):
    return lax.optimization_barrier(values.astype(jnp.bfloat16)).astype(jnp.float32)


def gated_linear(query_rows, key_rows, value_rows, fading_typical_span):
    length, head_count, key_width = query_rows.shape
    blocks = length // BLOCK
    query_rows = query_rows.reshape(blocks, BLOCK, head_count, key_width)
    key_rows = key_rows.reshape(blocks, BLOCK, head_count, key_width)
    value_rows = value_rows.reshape(blocks, BLOCK, head_count, -1)
    cumulative = jnp.cumsum(
        fading_typical_span.reshape(blocks, BLOCK, head_count, key_width), axis=1
    )
    tail_decay = cumulative[:, -1]
    query_in = query_rows * jnp.exp(cumulative)
    key_in = key_rows * jnp.exp(-cumulative)
    key_end = key_rows * jnp.exp(tail_decay[:, None] - cumulative)
    causal = jnp.tril(jnp.ones((BLOCK, BLOCK), dtype=bool))
    scores = jnp.einsum("nthk,nshk->nhts", query_in, key_in, precision=careful_evaluation)
    scores = jnp.where(causal, scores, 0.0)
    inner = jnp.einsum("nhts,nshv->nthv", scores, value_rows, precision=careful_evaluation)
    states = jnp.einsum("nshk,nshv->nhkv", key_end, value_rows, precision=careful_evaluation)

    def combine(earlier, latter):
        return (earlier[0] * latter[0], latter[0][..., None] * earlier[1] + latter[1])

    running = lax.associative_scan(combine, (jnp.exp(tail_decay), states))[1]
    carried = jnp.concatenate([jnp.zeros_like(running[:1]), running[:-1]], axis=0)
    outer = jnp.einsum("nthk,nhkv->nthv", query_in, carried, precision=careful_evaluation)
    return (inner + outer).reshape(length, head_count, -1)


def causal_taps(values, kernel):
    tap_count = kernel.shape[0]
    length = values.shape[0]
    padded = jnp.pad(values, ((tap_count - 1, 0), (0, 0)))
    kernel = kernel.astype(jnp.float32)
    summed = kernel[0] * padded[0:length]
    for offset in range(1, tap_count):
        summed = summed + kernel[offset] * padded[offset : offset + length]
    return summed


def add_products(pieces, normed):
    return tuple(
        (jnp.dot(normed, shard_rows, preferred_element_type=jnp.float32) for shard_rows in pieces)
    )


def on_device(
    block_source_tensor,
    attend_initial_norm_gain,
    each_channel_group_norm,
    attend_final_norm_gain,
    dense_initial_norm_gain,
    dense_final_norm_gain,
    question_map,
    address_map,
    payload_weights_map,
    fading_left_factor,
    fading_right_factor,
    fading_valve_constant,
    sudden_fade_excess,
    combining_map,
    valve_map,
    widening_map,
    valve_conv_stencil,
    widening_conv_stencil,
    narrowing_map,
):
    length, own_columns = block_source_tensor.shape
    tp_index = lax.axis_index("tp")
    full_width = own_columns * lax.axis_size("tp")
    full_rows = gathered_copies(block_source_tensor, "tp", 1)
    normed = norm_rows(full_rows.astype(jnp.float32), attend_initial_norm_gain).astype(jnp.bfloat16)
    query_proj, key_proj, value_proj = add_products(
        in_one_piece((question_map, address_map, payload_weights_map), "fs", 0, 1), normed
    )
    head_count = each_channel_group_norm.shape[0]
    query_rows = rounded(query_proj).reshape(length, head_count, KEY_DIM) * KEY_DIM ** (-0.5)
    key_rows = rounded(key_proj).reshape(length, head_count, KEY_DIM)
    value_rows = rounded(value_proj).reshape(length, head_count, VALUE_DIM)
    fading_narrow_count = jnp.dot(normed, fading_left_factor, preferred_element_type=jnp.float32)
    fading_typical_span = (
        jax.nn.log_sigmoid(
            jnp.dot(fading_narrow_count, fading_right_factor, precision=careful_evaluation)
            + fading_valve_constant
        )
        / valve_steepness
        + sudden_fade_excess
    )
    mixed_heads = gated_linear(
        query_rows, key_rows, value_rows, fading_typical_span.reshape(length, head_count, KEY_DIM)
    )
    head_out = (
        norm_rows(mixed_heads, each_channel_group_norm)
        .astype(jnp.bfloat16)
        .reshape(length, head_count * VALUE_DIM)
    )
    partials = jnp.dot(
        head_out, gathered_copies(combining_map, "fs", 1), preferred_element_type=jnp.float32
    )
    mixed = sum_at_owner(partials.astype(jnp.bfloat16), "tp", 1)
    squares = of_everyone(jnp.sum(mixed * mixed, axis=1), "tp")
    own_gain = lax.dynamic_slice_in_dim(attend_final_norm_gain, tp_index * own_columns, own_columns)
    first = (
        block_source_tensor.astype(jnp.float32)
        + mixed * lax.rsqrt(squares / full_width + epsilon)[:, None] * own_gain
    ).astype(jnp.bfloat16)
    first_rows = gathered_copies(first, "tp", 1)
    ffn_in = norm_rows(first_rows.astype(jnp.float32), dense_initial_norm_gain).astype(jnp.bfloat16)
    gate_pre, up_pre = add_products(in_one_piece((valve_map, widening_map), "fs", 0, 1), ffn_in)
    hidden = (
        jax.nn.silu(causal_taps(gate_pre, valve_conv_stencil))
        * causal_taps(up_pre, widening_conv_stencil)
    ).astype(jnp.bfloat16)
    down_partials = jnp.dot(
        hidden,
        lax.all_gather(narrowing_map, "fs", axis=1, tiled=True),
        preferred_element_type=jnp.float32,
    )
    channel = sum_at_owner(down_partials.astype(jnp.bfloat16), "tp", 1)
    channel_squares = of_everyone(jnp.sum(channel * channel, axis=1), "tp")
    own_post = lax.dynamic_slice_in_dim(dense_final_norm_gain, tp_index * own_columns, own_columns)
    return (
        first.astype(jnp.float32)
        + channel * lax.rsqrt(channel_squares / full_width + epsilon)[:, None] * own_post
    ).astype(jnp.bfloat16)


def solution(mesh):
    placed = (
        P(("grp", "fs"), "tp"),
        P(),
        P("tp", None),
        P(),
        P(),
        P(),
        P("fs", "tp"),
        P("fs", "tp"),
        P("fs", "tp"),
        P(),
        P(None, "tp"),
        P("tp"),
        P(("grp", "fs"), "tp"),
        P("tp", "fs"),
        P("fs", "tp"),
        P("fs", "tp"),
        P(None, "tp"),
        P(None, "tp"),
        P("tp", "fs"),
    )
    return jax.shard_map(
        on_device, mesh=mesh, in_specs=placed, out_specs=P(("grp", "fs"), "tp"), check_vma=False
    )
```

profile of v0, /device:TPU:33, one launch (start us, length us, event | category | flops | bytes accessed | tf_op | source)
XLA Modules:
  0.0 359.5 jit_solution(11381675309962298518)
XLA Ops:
  10.8 24.1 %all-to-all-start = ((bf16[8,512,256]{1,2,0:T(8,128)(2,1)}), bf16[8,512,256]{1,2,0:T(8,128)(2,1)S(1)}, u32[]{:S(2)}, u32[]{:S(2)}) async-start(bf16[8,512,256]{1,2,0:T(8,128)(2,1)} %broadcast_in_dim.20), calls=%async_computation | async-start | bytes 4194304 | tf_op jit(solution)/shard_map/all_to_all | solution.py:18
  35.8 25.4 %all-to-all-done = bf16[8,512,256]{1,2,0:T(8,128)(2,1)S(1)} async-done(((bf16[8,512,256]{1,2,0:T(8,128)(2,1)}), bf16[8,512,256]{1,2,0:T(8,128)(2,1)S(1)}, u32[]{:S(2)}, u32[]{:S(2)}) %all-to-all-start) | async-done | bytes 2097184 | tf_op jit(solution)/shard_map/all_to_all | solution.py:18
  62.2 5.8 %all-to-all-start.1 = ((bf16[16,256,128]{1,2,0:T(8,128)(2,1)}), bf16[16,256,128]{1,2,0:T(8,128)(2,1)}, u32[]{:S(2)}, u32[]{:S(2)}) async-start(bf16[16,256,128]{1,2,0:T(8,128)(2,1)} %broadcast_in_dim.23), calls=%async_computation.1 | async-start | bytes 2097152 | tf_op jit(solution)/shard_map/all_to_all | solution.py:18
  72.5 42.6 %all-gather.4.cloned.1.call-done = bf16[2048,512]{1,0:T(8,128)(2,1)} async-done(((bf16[128,512]{1,0:T(8,128)(2,1)}), bf16[2048,512]{1,0:T(8,128)(2,1)}) %all-gather.4.cloned.1.call-update) | async-done | bytes 2097168 | tf_op jit(solution)/shard_map/all_gather | solution.py:38
  115.2 2.8 convolution_convert_fusion.2
  130.4 3.9 %pad.46 = f32[16,1,128,256]{3,2,0,1:T(8,128)S(1)} pad(f32[8,1,128,256]{3,2,0,1:T(8,128)} %add.173, f32[]{:T(128)} %constant.14.clone.1), padding=1_0_1x0_0_0x0_0_0x0_0_0 | pad | bytes 3145732 | tf_op jit(solution)/shard_map/pad | solution.py:91
  136.1 4.1 %pad.45 = f32[16,1,128,256]{3,2,0,1:T(8,128)} pad(f32[8,1,128,256]{3,2,0,1:T(8,128)S(1)} %pad_maximum_fusion.1, f32[]{:T(128)} %constant.14.clone.1), padding=0_1_1x0_0_0x0_0_0x0_0_0 | pad | bytes 3145732 | tf_op jit(solution)/shard_map/pad | solution.py:91
  140.2 3.3 add.175
  146.6 11.5 %pad.65 = f32[31,1,128,256]{3,2,0,1:T(8,128)} pad(f32[16,1,128,256]{3,2,0,1:T(8,128)} %pad_maximum_fusion, f32[]{:T(128)} %constant.14.clone.1), padding=0_0_1x0_0_0x0_0_0x0_0_0 | pad | bytes 6160388 | tf_op jit(solution)/shard_map/slice | solution.py:92
  158.1 7.4 %pad.96 = f32[32,1,128,256]{3,2,0,1:T(8,128)} pad(f32[16,1,128,256]{3,2,0,1:T(8,128)S(1)} %copy-done.8, f32[]{:T(128)} %constant.14.clone.1), padding=1_0_1x0_0_0x0_0_0x0_0_0 | pad | bytes 6291460
  166.7 4.0 %slice_add_fusion.5 = f32[31,1,128,256]{3,2,0,1:T(8,128)S(1)} fusion(f32[31,1,128,256]{3,2,0,1:T(8,128)} %pad.65, f32[32,1,128,256]{3,2,0,1:T(8,128)} %pad.96), kind=kLoop, calls=%fused_computation.113 | loop fusion | flops 1015808 | bytes 12189696 | tf_op jit(solution)/shard_map/add | solution.py:91
  170.8 2.5 fusion.20
  175.5 42.1 %all_to_all.37 = bf16[8,512,256]{2,1,0:T(8,128)(2,1)S(1)} all-to-all(bf16[8,512,256]{2,1,0:T(8,128)(2,1)S(1)} %bitcast.106), channel_id=1, replica_groups=mesh['grp'=2,'fs'=16,'tp'=8] {'tp'}, dimensions={0} | all-to-all | bytes 4194304 | tf_op jit(solution)/shard_map/all_to_all | solution.py:48
  218.7 4.3 %all-to-all-start.3 = ((f32[8,1,512]{2,1,0:T(1,128)}), f32[8,1,512]{2,1,0:T(1,128)S(1)}, u32[]{:S(2)}, u32[]{:S(2)}) async-start(f32[8,1,512]{2,1,0:T(1,128)} %broadcast_in_dim.24), calls=%async_computation.3 | async-start | bytes 32768 | tf_op jit(solution)/shard_map/all_to_all | solution.py:18
  223.8 4.0 %all-to-all-done.3 = f32[8,1,512]{2,1,0:T(1,128)S(1)} async-done(((f32[8,1,512]{2,1,0:T(1,128)}), f32[8,1,512]{2,1,0:T(1,128)S(1)}, u32[]{:S(2)}, u32[]{:S(2)}) %all-to-all-start.3) | async-done | bytes 16416 | tf_op jit(solution)/shard_map/all_to_all | solution.py:18
  229.6 4.4 %all-to-all-start.4 = ((bf16[8,512,256]{1,2,0:T(8,128)(2,1)}), bf16[8,512,256]{1,2,0:T(8,128)(2,1)S(1)}, u32[]{:S(2)}, u32[]{:S(2)}) async-start(bf16[8,512,256]{1,2,0:T(8,128)(2,1)} %broadcast_in_dim.25), calls=%async_computation.4 | async-start | bytes 4194304 | tf_op jit(solution)/shard_map/all_to_all | solution.py:18
  234.8 25.4 %all-to-all-done.4 = bf16[8,512,256]{1,2,0:T(8,128)(2,1)S(1)} async-done(((bf16[8,512,256]{1,2,0:T(8,128)(2,1)}), bf16[8,512,256]{1,2,0:T(8,128)(2,1)S(1)}, u32[]{:S(2)}, u32[]{:S(2)}) %all-to-all-start.4) | async-done | bytes 2097184 | tf_op jit(solution)/shard_map/all_to_all | solution.py:18
  262.7 3.5 fusion.8
  266.2 3.6 fusion.10
  269.8 26.0 %all-gather.8.cloned.1.call-done = bf16[384,2048]{1,0:T(8,128)(2,1)} async-done(((bf16[384,128]{1,0:T(8,128)(2,1)}), bf16[384,2048]{1,0:T(8,128)(2,1)}) %all-gather.8.cloned.1.call-update) | async-done | bytes 1572880 | tf_op jit(solution)/shard_map/all_gather | solution.py:183
  295.8 3.9 %convolution_convert_fusion.1 = bf16[512,2048]{1,0:T(8,128)(2,1)S(1)} fusion(bf16[384,2048]{1,0:T(8,128)(2,1)} %all-gather.8.cloned.1.call-done, f32[512,384]{1,0:T(8,128)S(1)} %fusion.8, f32[512,384]{1,0:T(8,128)} %fusion.10, f32[384]{0:T(512)S(1)} %get-tuple-element.9, f32[384]{0:T(512)S(1)} %get-tuple-element.10, f32[384]{0:T(512)S(1)} %get-tuple-element.8, ...), kind=kOutput, calls=%fused_computation.14 | convolution fusion | flops 809500672 | bytes 5252096 | tf_op jit(solution)/shard_map/dot_general | solution.py:181
  299.9 42.2 %all_to_all.38 = bf16[8,512,256]{2,1,0:T(8,128)(2,1)S(1)} all-to-all(bf16[8,512,256]{2,1,0:T(8,128)(2,1)S(1)} %bitcast.107), channel_id=1, replica_groups=mesh['grp'=2,'fs'=16,'tp'=8] {'tp'}, dimensions={0} | all-to-all | bytes 4194304 | tf_op jit(solution)/shard_map/all_to_all | solution.py:48
  343.1 4.3 %all-to-all-start.6 = ((f32[8,1,512]{2,1,0:T(1,128)}), f32[8,1,512]{2,1,0:T(1,128)S(1)}, u32[]{:S(2)}, u32[]{:S(2)}) async-start(f32[8,1,512]{2,1,0:T(1,128)} %broadcast_in_dim.26), calls=%async_computation.6 | async-start | bytes 32768 | tf_op jit(solution)/shard_map/all_to_all | solution.py:18
  348.1 4.0 %all-to-all-done.6 = f32[8,1,512]{2,1,0:T(1,128)S(1)} async-done(((f32[8,1,512]{2,1,0:T(1,128)}), f32[8,1,512]{2,1,0:T(1,128)S(1)}, u32[]{:S(2)}, u32[]{:S(2)}) %all-to-all-start.6) | async-done | bytes 16416 | tf_op jit(solution)/shard_map/all_to_all | solution.py:18
  (154 shorter events, 40.9 us)
Async XLA Ops:
  6.5 64.0 %copy-start = (bf16[2048,16]{0,1:T(8,128)(2,1)S(1)}, bf16[2048,16]{0,1:T(8,128)(2,1)}, u32[]{:S(2)}) copy-start(bf16[2048,16]{0,1:T(8,128)(2,1)} %param.28) | copy-start | bytes 196612
  6.6 108.6 %all-gather.4.cloned.1.call-start = ((), (), s32[]{:S(2)}) async-start(), calls=%async_computation.7 | async-start | bytes 2228224 | tf_op jit(solution)/shard_map/all_gather | solution.py:38
  10.8 24.1 %copy-start.16 = (bf16[128,384]{1,0:T(8,128)(2,1)S(1)}, bf16[128,384]{1,0:T(8,128)(2,1)}, u32[]{:S(2)}) copy-start(bf16[128,384]{1,0:T(8,128)(2,1)} %param.34) | copy-start | bytes 294916
  10.8 24.1 %copy-start.17 = (bf16[128,384]{1,0:T(8,128)(2,1)S(1)}, bf16[128,384]{1,0:T(8,128)(2,1)}, u32[]{:S(2)}) copy-start(bf16[128,384]{1,0:T(8,128)(2,1)} %param.33) | copy-start | bytes 294916
  10.8 24.8 %copy-start.18 = (bf16[256,128]{1,0:T(8,128)(2,1)S(1)}, bf16[256,128]{1,0:T(8,128)(2,1)}, u32[]{:S(2)}) copy-start(bf16[256,128]{1,0:T(8,128)(2,1)} %param.32) | copy-start | bytes 196612
  10.8 50.4 %all-to-all-start = ((bf16[8,512,256]{1,2,0:T(8,128)(2,1)}), bf16[8,512,256]{1,2,0:T(8,128)(2,1)S(1)}, u32[]{:S(2)}, u32[]{:S(2)}) async-start(bf16[8,512,256]{1,2,0:T(8,128)(2,1)} %broadcast_in_dim.20), calls=%async_computation | async-start | bytes 4194304 | tf_op jit(solution)/shard_map/all_to_all | solution.py:18
  34.9 227.9 %all-gather.6.cloned.1.call-start = ((), (), s32[]{:S(2)}) async-start(), calls=%async_computation.8 | async-start | bytes 3342336 | tf_op jit(solution)/shard_map/all_gather | solution.py:38
  62.2 6.4 %copy-start.19 = (f32[2048]{0:T(1024)S(1)}, f32[2048]{0:T(1024)}, u32[]{:S(2)}) copy-start(f32[2048]{0:T(1024)} %param.20) | copy-start | bytes 24580
  62.2 111.1 %all-to-all-start.1 = ((bf16[16,256,128]{1,2,0:T(8,128)(2,1)}), bf16[16,256,128]{1,2,0:T(8,128)(2,1)}, u32[]{:S(2)}, u32[]{:S(2)}) async-start(bf16[16,256,128]{1,2,0:T(8,128)(2,1)} %broadcast_in_dim.23), calls=%async_computation.1 | async-start | bytes 2097152 | tf_op jit(solution)/shard_map/all_to_all | solution.py:18
  72.5 45.4 %copy-start.10 = (bf16[512,2048]{0,1:T(8,128)(2,1)S(1)}, bf16[512,2048]{0,1:T(8,128)(2,1)}, u32[]{:S(2)}) copy-start(bf16[512,2048]{0,1:T(8,128)(2,1)} %copy-done.9) | copy-start | bytes 6291460
  140.2 4.3 %copy-start.5 = (f32[16,1,128,256]{3,2,0,1:T(8,128)S(1)}, f32[16,1,128,256]{3,2,0,1:T(8,128)}, u32[]{:S(2)}) copy-start(f32[16,1,128,256]{3,2,0,1:T(8,128)} %pad.45) | copy-start | bytes 6291460
  146.6 11.5 %copy-start.8 = (f32[16,1,128,256]{3,2,0,1:T(8,128)S(1)}, f32[16,1,128,256]{3,2,0,1:T(8,128)}, u32[]{:S(2)}) copy-start(f32[16,1,128,256]{3,2,0,1:T(8,128)} %add.175) | copy-start | bytes 6291460
  158.1 7.5 %copy-start.12 = (f32[32,16,128]{2,0,1:T(8,128)S(1)}, f32[32,16,128]{2,0,1:T(8,128)}, u32[]{:S(2)}) copy-start(f32[32,16,128]{2,0,1:T(8,128)} %get-tuple-element.14) | copy-start | bytes 786436
  158.1 8.3 %copy-start.15 = (bf16[512,256]{1,0:T(8,128)(2,1)S(1)}, bf16[512,256]{1,0:T(8,128)(2,1)}, u32[]{:S(2)}) copy-start(bf16[512,256]{1,0:T(8,128)(2,1)} %copy-done.14) | copy-start | bytes 786436
  217.7 10.1 %copy-start.13 = (bf16[512,256]{1,0:T(8,128)(2,1)S(1)}, bf16[512,256]{1,0:T(8,128)(2,1)}, u32[]{:S(2)}) copy-start(bf16[512,256]{1,0:T(8,128)(2,1)} %param.19) | copy-start | bytes 786436
  218.7 9.0 %all-to-all-start.3 = ((f32[8,1,512]{2,1,0:T(1,128)}), f32[8,1,512]{2,1,0:T(1,128)S(1)}, u32[]{:S(2)}, u32[]{:S(2)}) async-start(f32[8,1,512]{2,1,0:T(1,128)} %broadcast_in_dim.24), calls=%async_computation.3 | async-start | bytes 32768 | tf_op jit(solution)/shard_map/all_to_all | solution.py:18
  229.6 5.1 %copy-start.21 = (bf16[3,384]{1,0:T(4,128)(2,1)S(1)}, bf16[3,384]{1,0:T(4,128)(2,1)}, u32[]{:S(2)}) copy-start(bf16[3,384]{1,0:T(4,128)(2,1)} %param.36) | copy-start | bytes 6916
  229.6 5.1 %copy-start.22 = (bf16[3,384]{1,0:T(4,128)(2,1)S(1)}, bf16[3,384]{1,0:T(4,128)(2,1)}, u32[]{:S(2)}) copy-start(bf16[3,384]{1,0:T(4,128)(2,1)} %param.35) | copy-start | bytes 6916
  229.6 30.7 %all-to-all-start.4 = ((bf16[8,512,256]{1,2,0:T(8,128)(2,1)}), bf16[8,512,256]{1,2,0:T(8,128)(2,1)S(1)}, u32[]{:S(2)}, u32[]{:S(2)}) async-start(bf16[8,512,256]{1,2,0:T(8,128)(2,1)} %broadcast_in_dim.25), calls=%async_computation.4 | async-start | bytes 4194304 | tf_op jit(solution)/shard_map/all_to_all | solution.py:18
  234.0 26.8 %copy-start.20 = (f32[2048]{0:T(1024)S(1)}, f32[2048]{0:T(1024)}, u32[]{:S(2)}) copy-start(f32[2048]{0:T(1024)} %param.23) | copy-start | bytes 24580
  234.0 61.8 %all-gather.8.cloned.1.call-start = ((), (), s32[]{:S(2)}) async-start(), calls=%async_computation.9 | async-start | bytes 1671168 | tf_op jit(solution)/shard_map/all_gather | solution.py:183
  262.7 3.5 copy-start.4
  299.8 53.2 %copy-start.1 = (bf16[2048,16]{0,1:T(8,128)(2,1)S(1)}, bf16[2048,16]{0,1:T(8,128)(2,1)}, u32[]{:S(2)}) copy-start(bf16[2048,16]{0,1:T(8,128)(2,1)} %param.28) | copy-start | bytes 196612
  343.1 9.0 %all-to-all-start.6 = ((f32[8,1,512]{2,1,0:T(1,128)}), f32[8,1,512]{2,1,0:T(1,128)S(1)}, u32[]{:S(2)}, u32[]{:S(2)}) async-start(f32[8,1,512]{2,1,0:T(1,128)} %broadcast_in_dim.26), calls=%async_computation.6 | async-start | bytes 32768 | tf_op jit(solution)/shard_map/all_to_all | solution.py:18
  (13 other events, 22.6 us)
Sparse Core Ops, SparseCore 0:
  9.1 105.9 all-gather.3
  117.0 73.0 all-gather.5
  236.5 59.2 all-gather.7
where the time goes:
time: 361 us; the launch traced here: 360 us
  waiting for transfers between devices  128 us (35%)
  blocking collectives  84.3 us (23%)
  local copies, waits for them, and re-layouts  43.5 us (12%)
  starting transfers between devices  42.8 us (12%)
  matrix products  23.7 us (7%)
  other arithmetic  23.3 us (6%)
  between operations  13.7 us (4%)
    all_to_all x2, blocking collectives, sum_at_owner(): lax.all_to_all(tiles, axis, split_axis=0, concat_axis=0, tiled=True)  84.3 us
    all_to_all x5, waiting for transfers between devices, copy_for_each(): return lax.all_to_all(copies, axis, split_axis=0, concat_axis=0, tiled=True)  58.7 us
    all_to_all x5, starting transfers between devices, copy_for_each(): return lax.all_to_all(copies, axis, split_axis=0, concat_axis=0, tiled=True)  42.8 us
    all_gather x2, waiting for transfers between devices, in_one_piece(): lax.all_gather(both, axis, axis=dim, tiled=True)  42.6 us
    all_gather x1, waiting for transfers between devices, on_device(): lax.all_gather(narrowing_map, 'fs', axis=1, tiled=True)  26 us
    unnamed x59, local copies, waits for them, and re-layouts  16 us
    slice x1, local copies, waits for them, and re-layouts, gated_linear(): running[:-1]  11.5 us
    dot_general x5, matrix products, add_products(): jnp.dot(normed, shard_rows, preferred_element_type=jnp.float32)  11.4 us
  transfers between devices with their start and end apart: 8, of which 6 were waited for; matrix products, arithmetic and copies ran while one was open for 21% of the time, Pallas kernels for 0%

commit v1 on v0

v1 whole, which is shorter than its diff:
```python
import functools

import jax
import jax.numpy as jnp
from jax import lax
from jax.experimental import pallas as pl
from jax.experimental.pallas import tpu as pltpu
from jax.sharding import PartitionSpec as P

EPS = 1e-06
STEEPNESS = 16.0
MESH = pl.DeviceIdType.MESH
F32 = jnp.float32
BF16 = jnp.bfloat16
NEG = -1e30


def mm(a, b):
    return jnp.dot(a, b, preferred_element_type=F32)


def mm_nt(a, b):
    return lax.dot_general(a, b, (((1,), (1,)), ((), ())), preferred_element_type=F32)


def split2(v):
    hi = v.astype(BF16)
    return hi, (v - hi.astype(F32)).astype(BF16)


def layer_kernel(
    dims,
    x_hbm, q_hbm, k_hbm, v_hbm, comb_hbm, gate_hbm, up_hbm, down_hbm, exc_hbm,
    g1_ref, gaf_ref, gdi_ref, gdf_ref, egn_ref, left_ref, right_ref, const_ref, tapg_ref, tapu_ref,
    out_ref,
    xb, X, XG, F, wqkv, wc, wgu, wd, exc, ss, hout, hidden, G, firstb, acc, so, si, o2, orr, oll, ih, ifl,
    local_sem, zrecv, zsend, yrecv, ysend, agrecv, agsend, ssrecv, sssend, sibrecv, sibsend, rsrecv, rssend,
):
    NG, NZ, NTP = dims
    T, OC = xb.shape
    D = X.shape[1]
    NX = NTP // 2
    KD = q_hbm.shape[1]
    VD = v_hbm.shape[1]
    FU = gate_hbm.shape[1]
    RZ = q_hbm.shape[0]
    CZ = comb_hbm.shape[1]
    PER = OC // CZ
    H = T // 2
    HALF = NZ // 2

    g, z, t = lax.axis_index("grp"), lax.axis_index("fs"), lax.axis_index("tp")
    par = lax.rem(g, 2)
    pg = g + 1 - 2 * par
    xi, c = t // 2, lax.rem(t, 2)
    chip_r, chip_l, chip_2 = lax.rem(xi + 1, NX), lax.rem(xi + NX - 1, NX), lax.rem(xi + 2, NX)
    sib = 2 * xi + 1 - c
    tr, tl = 2 * chip_r + c, 2 * chip_l + c
    zr, zl = lax.rem(z + 1, NZ), lax.rem(z + NZ - 1, NZ)

    def m(v, n):
        return pl.multiple_of(v, n)

    def wview(ref, o, r0, rows):
        return ref.at[pl.ds(m(o * RZ + r0, 16), rows), :]

    def cview(ref, o, r0, rows):
        return ref.at[o // PER, pl.ds(m(r0, 16), rows), pl.ds(m(lax.rem(o, PER) * CZ, CZ), CZ)]

    def guview(o, r0, rows, c0, cols):
        return wgu.at[pl.ds(m(o * RZ + r0, 16), rows), pl.ds(m(c0, 128), cols)]

    VR = comb_hbm.shape[0]
    b_m, b_c = 80, VR - 160
    c_m = 2 * FU // 3
    d_m = FU // 3
    PHASES = {
        "A": [(lambda o, p, i=i: wview(wqkv, o, p * 48 + 16 * i, 16), True) for i in range(3)]
        + [(lambda o, p, i=i: wview(wqkv, o, 96 + 16 * i, 16), False) for i in range((RZ - 96) // 16)],
        "B": [
            (lambda o, p: cview(wc, o, p * b_m, b_m), True),
            (lambda o, p: cview(wc, o, 2 * b_m, b_c), False),
        ],
        "P": [
            (lambda o, p: guview(o, 0, RZ // 2, p * c_m, c_m), True),
            (lambda o, p: guview(o, 0, RZ // 2, 2 * c_m, c_m), False),
        ],
        "Q": [
            (lambda o, p: guview(o, RZ // 2, RZ // 2, p * c_m, c_m), True),
            (lambda o, p: guview(o, RZ // 2, RZ // 2, 2 * c_m, c_m), False),
        ],
        "D": [
            (lambda o, p: cview(wd, o, p * d_m, d_m), True),
            (lambda o, p: cview(wd, o, 2 * d_m, d_m), False),
        ],
    }
    ANTIPODE = {"A": ((0, 2, 4), (1, 3)), "B": ((0,), (1,)), "P": ((0,), (1,)), "Q": ((1,), (0,)), "D": ((0,), (1,))}
    ZBASE, YBASE, zn, yn = {}, {}, 0, 0
    for name, chunks in PHASES.items():
        ZBASE[name], YBASE[name] = zn, yn
        zn += len(chunks)
        yn += sum(e for _, e in chunks)
    pending_z, pending_y = {}, {}

    def zcopy(phase, ci, d, hop):
        o = lax.rem(z + NZ - hop, NZ) if d == 0 else lax.rem(z + hop, NZ)
        view = PHASES[phase][ci][0](o, par)
        return pltpu.make_async_remote_copy(
            src_ref=view, dst_ref=view,
            send_sem=zsend.at[d, ZBASE[phase] + ci, hop % 2],
            recv_sem=zrecv.at[d, ZBASE[phase] + ci, hop],
            device_id={"fs": zr if d == 0 else zl}, device_id_type=MESH,
        )

    def zstart(phase, ci, d, hop):
        key = (d, ZBASE[phase] + ci, hop % 2)
        if key in pending_z:
            pending_z.pop(key).wait_send()
        copy = zcopy(phase, ci, d, hop)
        copy.start()
        pending_z[key] = copy

    def zwait(phase, ci, d, s):
        o = lax.rem(z + NZ - s, NZ) if d == 0 else lax.rem(z + s, NZ)
        view = PHASES[phase][ci][0](o, par)
        pltpu.make_async_remote_copy(
            src_ref=view, dst_ref=view,
            send_sem=zsend.at[d, ZBASE[phase] + ci, 0],
            recv_sem=zrecv.at[d, ZBASE[phase] + ci, s - 1],
            device_id={"fs": zr if d == 0 else zl}, device_id_type=MESH,
        ).wait_recv()

    def ycopy(phase, ci, d, s, p):
        yi = YBASE[phase] + [i for i, (_, e) in enumerate(PHASES[phase]) if e].index(ci)
        rel = (NZ - s) % NZ if d == 0 else s
        o = lax.rem(z + rel, NZ)
        view = PHASES[phase][ci][0](o, p)
        return yi, pltpu.make_async_remote_copy(
            src_ref=view, dst_ref=view,
            send_sem=ysend.at[yi, d, s % 2],
            recv_sem=yrecv.at[yi, rel],
            device_id={"grp": pg}, device_id_type=MESH,
        )

    def ystart(phase, ci, d, s):
        yi, copy = ycopy(phase, ci, d, s, par)
        key = (yi, d, s % 2)
        if key in pending_y:
            pending_y.pop(key).wait_send()
        copy.start()
        pending_y[key] = copy

    def own_sends(phase):
        for ci in range(len(PHASES[phase])):
            for d in (0, 1):
                zstart(phase, ci, d, 0)

    deferred = []

    def y_flush():
        for args in deferred:
            ystart(*args)
        deferred.clear()

    def tick(phase, s, hold=False):
        for ci, (_, exchanged) in enumerate(PHASES[phase]):
            for d in (0, 1):
                if s == HALF and ci not in ANTIPODE[phase][d]:
                    continue
                zwait(phase, ci, d, s)
                if s < HALF - 1 or (s == HALF - 1 and ci in ANTIPODE[phase][d]):
                    zstart(phase, ci, d, s)
                if exchanged and hold:
                    deferred.append((phase, ci, d, s))
                elif exchanged:
                    ystart(phase, ci, d, s)

    def y_all(phase):
        for s in range(1, HALF + 1):
            for ci, (_, exchanged) in enumerate(PHASES[phase]):
                if exchanged:
                    for d in (0, 1):
                        if s == HALF and ci not in ANTIPODE[phase][d]:
                            continue
                        ycopy(phase, ci, d, s, 1 - par)[1].wait_recv()

    zo = z
    locals_ = [
        (x_hbm, X.at[:, pl.ds(m(t * OC, OC), OC)]),
        (q_hbm, wqkv.at[pl.ds(m(zo * RZ, 16), RZ), 0:KD]),
        (k_hbm, wqkv.at[pl.ds(m(zo * RZ, 16), RZ), KD : 2 * KD]),
        (v_hbm, wqkv.at[pl.ds(m(zo * RZ, 16), RZ), 2 * KD : 2 * KD + VD]),
        (comb_hbm, cview(wc, zo, 0, VR)),
        (gate_hbm, wgu.at[pl.ds(m(zo * RZ, 16), RZ), 0:FU]),
        (up_hbm, wgu.at[pl.ds(m(zo * RZ, 16), RZ), FU : 2 * FU]),
        (down_hbm, cview(wd, zo, 0, FU)),
        (exc_hbm, exc),
        (x_hbm, xb),
    ]
    loads = [pltpu.make_async_copy(a, b, local_sem.at[i]) for i, (a, b) in enumerate(locals_)]
    for copy in loads:
        copy.start()

    barrier = pltpu.get_barrier_semaphore()
    for d in range(1, NTP):
        pl.semaphore_signal(barrier, inc=1, device_id={"tp": lax.rem(t + d, NTP)}, device_id_type=MESH)
    for other in (zr, zl):
        pl.semaphore_signal(barrier, inc=1, device_id={"fs": other}, device_id_type=MESH)
    pl.semaphore_signal(barrier, inc=1, device_id={"grp": pg}, device_id_type=MESH)
    for i in range(0, 4):
        loads[i].wait()
    pl.semaphore_wait(barrier, NTP + 2)
    own_sends("A")

    row_iota = lax.broadcasted_iota(jnp.int32, (T, 1), 0)
    lane_iota = lax.broadcasted_iota(jnp.int32, (128, 128), 1)

    def gain_row(ref):
        per = OC // 128
        rows = [ref[pl.ds(t * per + i, 1), :] for i in range(per)]
        return jnp.concatenate(rows, axis=1)

    pending = []

    NB = T // 128

    def ss_send(k, cols):
        mat = jnp.zeros((128, 128), F32)
        for i, col in enumerate(cols):
            for j in range(NB):
                mat = jnp.where(lane_iota == i * NB + j, col[j * 128 : (j + 1) * 128], mat)
        ss[k, t] = mat.T[0:16, :]
        for d in range(1, NTP):
            copy = pltpu.make_async_remote_copy(
                src_ref=ss.at[k, t], dst_ref=ss.at[k, t],
                send_sem=sssend.at[k, d], recv_sem=ssrecv.at[k, d],
                device_id={"tp": lax.rem(t + d, NTP)}, device_id_type=MESH,
            )
            copy.start()
            pending.append(copy)

    def ss_total(k):
        for d in range(1, NTP):
            src = ss.at[k, lax.rem(t + NTP - d, NTP)]
            pltpu.make_async_remote_copy(
                src_ref=src, dst_ref=src, send_sem=sssend.at[k, d], recv_sem=ssrecv.at[k, d],
                device_id={"tp": lax.rem(t + d, NTP)}, device_id_type=MESH,
            ).wait_recv()
        total = ss[k, 0]
        for i in range(1, NTP):
            total = total + ss[k, i]
        return total

    def columns(rows):
        cols = jnp.concatenate([rows, jnp.zeros((120, 128), F32)], axis=0).T
        pick = lambda a: jnp.concatenate([cols[:, a + j : a + j + 1] for j in range(NB)], axis=0)
        return pick(0), pick(NB)

    def scale_into(ref, lo, hi):
        for l in range(lo, hi):
            cols = slice(l * 128, (l + 1) * 128)
            XG[:, cols] = (X[:, cols].astype(F32) * ref[l : l + 1, :]).astype(BF16)

    def part(buf, o, h):
        return buf.at[pl.ds(h * H, H), pl.ds(m(o * OC, OC), OC)]

    def ag_copy(buf, k, slot, o, h, dev):
        view = part(buf, o, h)
        return pltpu.make_async_remote_copy(
            src_ref=view, dst_ref=view, send_sem=agsend.at[k, slot], recv_sem=agrecv.at[k, slot],
            device_id={"tp": dev}, device_id_type=MESH,
        )

    def ag_start(buf, k):
        for slot, h, dev in ((0, 0, tr), (2, 1, tl), (1, 1, tr), (3, 0, tl), (6, 0, sib), (7, 1, sib)):
            copy = ag_copy(buf, k, slot, t, h, dev)
            copy.start()
            pending.append(copy)

    SRC = {0: (tl, 0), 1: (tl, 1), 2: (tr, 1), 3: (tr, 0), 4: (2 * chip_2 + c, 0), 5: (2 * chip_2 + c, 1)}

    def ag_take(buf, k, slots):
        for slot in slots:
            o, h = SRC[slot]
            ag_copy(buf, k, slot, o, h, sib).wait_recv()
            sends = [(slot + 8, sib)]
            if slot == 0:
                sends = [(4, tr)] + sends
            if slot == 2:
                sends = [(5, tl)] + sends
            for target, dev in sends:
                copy = ag_copy(buf, k, target, o, h, dev)
                copy.start()
                pending.append(copy)

    def ag_end(buf, k):
        for slot in (6, 7):
            ag_copy(buf, k, slot, sib, slot - 6, sib).wait_recv()
        for slot in range(6):
            o, h = SRC[slot]
            ag_copy(buf, k, slot + 8, o, h, sib).wait_recv()

    ag_start(X, 0)
    loads[9].wait()
    x32 = xb[...].astype(F32)
    ss_send(0, [jnp.sum(x32 * x32, axis=1, keepdims=True)])
    for i in range(4, 9):
        loads[i].wait()
    NL = D // 128

    tick("A", 1)
    own_sends("B")
    tick("A", 2)
    ag_take(X, 0, (0, 2))
    tick("A", 3)
    ag_take(X, 0, (1, 3))
    tick("B", 1, True)
    tick("A", 4)
    tick("B", 2, True)
    ag_take(X, 0, (4, 5))
    tick("A", 5)
    tick("B", 3, True)
    ag_end(X, 0)
    tick("A", 6)
    scale_into(g1_ref, 0, NL // 2)
    tick("B", 4, True)
    tick("A", 7)
    scale_into(g1_ref, NL // 2, NL)
    tick("B", 5, True)
    tick("A", 8)
    y_flush()
    tick("B", 6)
    own_sends("P")
    total0 = ss_total(0)
    r1, _ = columns(lax.rsqrt(total0[0:8] / D + EPS))
    y_all("A")

    qk = mm(XG[...], wqkv[:, 0 : 2 * KD]) * r1
    q = qk[:, 0:KD].astype(BF16).astype(F32) * KD ** (-0.5)
    k = qk[:, KD : 2 * KD].astype(BF16).astype(F32)
    v = (mm(XG[...], wqkv[:, 2 * KD : 2 * KD + VD]) * r1).astype(BF16)
    tick("B", 7)
    own_sends("Q")
    low = mm_nt(XG[...], left_ref[...]) * r1
    low_hi, low_lo = split2(low)
    right_hi, right_lo = split2(right_ref[...])
    pre = mm(low_hi, right_hi) + (mm(low_lo, right_hi) + mm(low_hi, right_lo)) + const_ref[...]
    ld = (jnp.minimum(pre, 0.0) - jnp.log1p(jnp.exp(-jnp.abs(pre)))) / STEEPNESS + exc[...]

    ri = lax.broadcasted_iota(jnp.int32, (128, 128), 0)
    tri = jnp.where(ri >= lane_iota, 1.0, 0.0).astype(BF16)
    ld_hi, ld_lo = split2(ld)
    pieces, carry = [], jnp.zeros((1, KD), F32)
    for j in range(T // 128):
        rows = slice(j * 128, (j + 1) * 128)
        run = mm(tri, ld_hi[rows]) + mm(tri, ld_lo[rows]) + carry
        carry = run[127:128]
        pieces.append(run)
    b = jnp.concatenate(pieces, axis=0)
    tick("B", 8)

    def offsets(span):
        b3 = b.reshape(T // span, span, KD)
        return (b3 - b3[:, span // 2 - 1 : span // 2, :]).reshape(T, KD)

    def level(span):
        d = offsets(span)
        second = lax.rem(row_iota, span) >= span // 2
        e = jnp.exp(jnp.where(second, d, -d))
        return jnp.where(second, q * e, 0.0).astype(BF16), jnp.where(second, 0.0, k * e).astype(BF16)

    dd = offsets(32)
    qd, kd = (q * jnp.exp(dd)).astype(BF16), (k * jnp.exp(-dd)).astype(BF16)
    q64, k64 = level(64)
    q128, k128 = level(128)
    q256, k256 = level(256)
    q512, k512 = level(512)
    tick("P", 1)
    ci_ = lane_iota
    in32 = (ri // 32 == ci_ // 32) & (ri >= ci_)
    in64 = (ri // 64 == ci_ // 64) & (ri // 32 != ci_ // 32)
    diag = []
    for j in range(T // 128):
        rows = slice(j * 128, (j + 1) * 128)
        s = jnp.where(in32, mm_nt(qd[rows], kd[rows]), 0.0)
        s = s + jnp.where(in64, mm_nt(q64[rows], k64[rows]), 0.0)
        s = s + mm_nt(q128[rows], k128[rows])
        diag.append(s.astype(BF16))
    zero128 = jnp.zeros((128, 128), BF16)
    halves = []
    for j in range(2):
        lo = slice(j * 256, j * 256 + 128)
        hi = slice(j * 256 + 128, (j + 1) * 256)
        cross = mm_nt(q256[hi], k256[lo]).astype(BF16)
        top = mm(diag[2 * j], v[lo])
        bottom = mm(jnp.concatenate([cross, diag[2 * j + 1]], axis=1), v[j * 256 : (j + 1) * 256])
        halves.append(jnp.concatenate([top, bottom], axis=0))
    far = mm_nt(q512[256:512], k512[0:256]).astype(BF16)
    heads = jnp.concatenate([halves[0], halves[1] + mm(far, v[0:256])], axis=0)
    hs = lax.rsqrt(jnp.mean(heads * heads, axis=1, keepdims=True) + EPS)
    hout[...] = (heads * hs * egn_ref[...]).astype(BF16)
    tick("Q", 1)
    own_sends("D")
    y_all("B")

    def rs(k, lhs_ref, w, between):
        sibs = []
        order = (chip_2, chip_r, chip_l, xi)

        def products(n):
            so[k, n] = mm(lhs_ref[...], w[2 * order[n] + 1 - c]).astype(BF16)
            copy = pltpu.make_async_remote_copy(
                src_ref=so.at[k, n], dst_ref=si.at[k, n], send_sem=sibsend.at[k, n], recv_sem=sibrecv.at[k, n],
                device_id={"tp": sib}, device_id_type=MESH,
            )
            copy.start()
            pending.append(copy)
            sibs.append(copy)
            acc[n] = mm(lhs_ref[...], w[2 * order[n] + c])

        def send(slot, src, dst, dev):
            copy = pltpu.make_async_remote_copy(
                src_ref=src, dst_ref=dst, send_sem=rssend.at[k, slot], recv_sem=rsrecv.at[k, slot],
                device_id={"tp": dev}, device_id_type=MESH,
            )
            copy.start()
            pending.append(copy)

        def take(slot, dst):
            pltpu.make_async_remote_copy(
                src_ref=dst, dst_ref=dst, send_sem=rssend.at[k, slot], recv_sem=rsrecv.at[k, slot],
                device_id={"tp": sib}, device_id_type=MESH,
            ).wait_recv()

        lo, hi = pl.ds(0, H), pl.ds(H, H)
        products(0)
        products(1)
        sibs[0].wait_recv()
        o2[k, lo, :] = (acc[0, lo, :] + si[k, 0, lo, :].astype(F32)).astype(BF16)
        send(0, o2.at[k, lo], ih.at[k, 0], tr)
        o2[k, hi, :] = (acc[0, hi, :] + si[k, 0, hi, :].astype(F32)).astype(BF16)
        send(1, o2.at[k, hi], ih.at[k, 1], tl)
        products(2)
        sibs[1].wait_recv()
        orr[k, hi, :] = (acc[1, hi, :] + si[k, 1, hi, :].astype(F32)).astype(BF16)
        send(2, orr.at[k, hi], ifl.at[k, 0, hi], tr)
        between(0)
        products(3)
        sibs[2].wait_recv()
        oll[k, lo, :] = (acc[2, lo, :] + si[k, 2, lo, :].astype(F32)).astype(BF16)
        send(4, oll.at[k, lo], ifl.at[k, 1, lo], tl)
        between(1)
        take(0, ih.at[k, 0])
        orr[k, lo, :] = (acc[1, lo, :] + si[k, 1, lo, :].astype(F32) + ih[k, 0].astype(F32)).astype(BF16)
        send(3, orr.at[k, lo], ifl.at[k, 0, lo], tr)
        take(1, ih.at[k, 1])
        oll[k, hi, :] = (acc[2, hi, :] + si[k, 2, hi, :].astype(F32) + ih[k, 1].astype(F32)).astype(BF16)
        send(5, oll.at[k, hi], ifl.at[k, 1, hi], tl)
        sibs[3].wait_recv()
        between(2)
        take(2, ifl.at[k, 0, hi])
        take(4, ifl.at[k, 1, lo])
        between(3)
        take(3, ifl.at[k, 0, lo])
        take(5, ifl.at[k, 1, hi])
        return acc[3] + si[k, 3].astype(F32) + (ifl[k, 0].astype(F32) + ifl[k, 1].astype(F32))

    def between0(i):
        if i == 0:
            tick("P", 2)
        elif i == 1:
            tick("Q", 2)
            tick("P", 3)
        elif i == 2:
            tick("Q", 3)
            tick("D", 1)
            scale_into(gdi_ref, 0, NL // 2)
            tick("P", 4)
        else:
            tick("Q", 4)
            scale_into(gdi_ref, NL // 2, NL)

    mixed = rs(0, hout, wc, between0)
    mg = mixed * gain_row(gaf_ref)
    F[:, pl.ds(m(t * OC, OC), OC)] = (mg * gain_row(gdi_ref)).astype(BF16)
    ag_start(F, 1)
    x32 = xb[...].astype(F32)
    ss_send(1, [jnp.sum(a, axis=1, keepdims=True) for a in (mixed * mixed, x32 * mg, mg * mg)])
    acc[3] = mg
    tick("P", 5)
    tick("D", 2)
    tick("Q", 5)
    ag_take(F, 1, (0, 2))
    tick("P", 6)
    tick("D", 3)
    tick("Q", 6)
    ag_take(F, 1, (1, 3))
    tick("P", 7)
    tick("D", 4)
    tick("Q", 7)
    ag_take(F, 1, (4, 5))
    tick("P", 8)
    tick("D", 5)
    tick("Q", 8)
    y_all("P")
    y_all("Q")
    PAD = 8
    G[0:PAD, :] = jnp.zeros((PAD, 2 * FU), F32)
    for n in range(2 * FU // 256):
        cols = slice(n * 256, (n + 1) * 256)
        G[PAD : PAD + T, cols] = mm(XG[...], wgu[:, cols])
    tick("D", 6)
    ag_end(F, 1)
    total1 = ss_total(1)
    ra_rows = lax.rsqrt(total1[0:NB] / D + EPS)
    squares = total0[0:NB] + 2.0 * ra_rows * total1[NB : 2 * NB] + ra_rows * ra_rows * total1[2 * NB : 3 * NB]
    ra, r2 = columns(jnp.concatenate([ra_rows, lax.rsqrt(squares / D + EPS)], axis=0))

    for n in range(2 * FU // 256):
        cols = slice(n * 256, (n + 1) * 256)
        G[PAD : PAD + T, cols] = (G[PAD : PAD + T, cols] + mm(F[...], wgu[:, cols]) * ra) * r2
    tick("D", 7)
    firstb[...] = (xb[...].astype(F32) + acc[3] * ra).astype(BF16)

    def taps(ref, base):
        w = ref[:, base % FU : base % FU + 128].astype(F32)
        n = w.shape[0]
        total = None
        for j in range(n):
            term = w[j : j + 1] * G[PAD - (n - 1) + j : PAD - (n - 1) + j + T, base : base + 128]
            total = term if total is None else total + term
        return total

    for n in range(FU // 128):
        gc, uc = taps(tapg_ref, n * 128), taps(tapu_ref, FU + n * 128)
        hidden[:, n * 128 : (n + 1) * 128] = (gc / (1.0 + jnp.exp(-gc)) * uc).astype(BF16)
    tick("D", 8)
    y_all("D")
    channel = rs(1, hidden, wd, lambda i: None)
    ss_send(3, [jnp.sum(channel * channel, axis=1, keepdims=True)])
    acc[3] = channel
    for copy in list(pending_z.values()) + list(pending_y.values()) + pending[: -(NTP - 1)]:
        copy.wait_send()
    rc, _ = columns(lax.rsqrt(ss_total(3)[0:8] / D + EPS))
    out_ref[...] = (firstb[...].astype(F32) + acc[3] * rc * gain_row(gdf_ref)).astype(BF16)
    for copy in pending[-(NTP - 1) :]:
        copy.wait_send()


def on_device(
    dims, x, g1, egn, gaf, gdi, gdf, wq, wk, wv, left, right, const, excess, comb, gate, up, tapg, tapu, down
):
    NG, NZ, NTP = dims
    T, OC = x.shape
    D = OC * NTP
    KD, VD, FU = wq.shape[1], wv.shape[1], gate.shape[1]
    any_ = pl.BlockSpec(memory_space=pl.ANY)
    vm = pl.BlockSpec(memory_space=pltpu.VMEM)
    DMA = pltpu.SemaphoreType.DMA
    NX = NTP // 2
    VM = pltpu.VMEM
    scratch = [
        VM((T, OC), BF16), VM((T, D), BF16), VM((T, D), BF16), VM((T, D), BF16),
        VM((D, 2 * KD + VD), BF16), VM((NTP, comb.shape[0], OC), BF16), VM((D, 2 * FU), BF16), VM((NTP, FU, OC), BF16),
        VM((T, KD), F32), VM((4, NTP, 16, 128), F32),
        VM((T, VD), BF16), VM((T, FU), BF16), VM((T + 8, 2 * FU), F32), VM((T, OC), BF16),
        VM((NX, T, OC), F32), VM((2, NX, T, OC), BF16), VM((2, NX, T, OC), BF16),
        VM((2, T, OC), BF16), VM((2, T, OC), BF16), VM((2, T, OC), BF16),
        VM((2, 2, T // 2, OC), BF16), VM((2, 2, T, OC), BF16),
        DMA((10,)), DMA((2, 13, NZ // 2)), DMA((2, 13, 2)), DMA((7, NZ)), DMA((7, 2, 2)),
        DMA((2, 14)), DMA((2, 14)), DMA((4, NTP)), DMA((4, NTP)), DMA((2, NX)), DMA((2, NX)), DMA((2, 6)), DMA((2, 6)),
    ]
    return pl.pallas_call(
        functools.partial(layer_kernel, dims),
        out_shape=jax.ShapeDtypeStruct((T, OC), BF16),
        in_specs=[any_] * 9 + [vm] * 10,
        out_specs=vm,
        scratch_shapes=scratch,
        compiler_params=pltpu.CompilerParams(
            collective_id=0, has_side_effects=True, vmem_limit_bytes=60 * 1024 * 1024
        ),
        name="layer",
    )(
        x, wq, wk, wv, comb, gate, up, down, excess,
        g1.reshape(-1, 128), gaf.reshape(-1, 128), gdi.reshape(-1, 128), gdf.reshape(-1, 128),
        egn, left.T, right, const.reshape(1, -1), tapg, tapu,
    )


def solution(mesh):
    dims = (mesh.shape["grp"], mesh.shape["fs"], mesh.shape["tp"])
    placed = (
        P(("grp", "fs"), "tp"), P(), P("tp", None), P(), P(), P(), P("fs", "tp"), P("fs", "tp"), P("fs", "tp"), P(),
        P(None, "tp"), P("tp"), P(("grp", "fs"), "tp"), P("tp", "fs"), P("fs", "tp"), P("fs", "tp"), P(None, "tp"),
        P(None, "tp"), P("tp", "fs"),
    )
    return jax.shard_map(
        functools.partial(on_device, dims), mesh=mesh, in_specs=placed, out_specs=P(("grp", "fs"), "tp"),
        check_vma=False,
    )
```

time: 361 us -> 134 us (0.37)
  Pallas kernels: 0 us -> 132 us
  waiting for transfers between devices: 128 us -> 0 us
  blocking collectives: 84.3 us -> 0 us
  starting transfers between devices: 42.8 us -> 0 us
  local copies, waits for them, and re-layouts: 43.5 us -> 1.67 us
  matrix products: 23.7 us -> 0 us
  other arithmetic: 23.3 us -> 0 us
  between operations: 13.7 us -> 0.01 us
    pallas_call x0 -> x1, Pallas kernels: none -> 132 us  [on_device(): pl.pallas_call(functools.partial(layer_kernel, dims), out_shape=jax.Shape...]
    all_to_all x2 -> x0, blocking collectives: 84.3 us -> none  [sum_at_owner(): lax.all_to_all(tiles, axis, split_axis=0, concat_axis=0, tiled=True)]
    all_gather x3 -> x0, waiting for transfers between devices: 68.6 us -> none  [the longest x2 42.6 us: in_one_piece(): lax.all_gather(both, axis, axis=dim, tiled=True)]
    all_to_all x5 -> x0, waiting for transfers between devices: 58.7 us -> none  [copy_for_each(): return lax.all_to_all(copies, axis, split_axis=0, concat_axis=0, tiled=True)]
    all_to_all x5 -> x0, starting transfers between devices: 42.8 us -> none  [copy_for_each(): return lax.all_to_all(copies, axis, split_axis=0, concat_axis=0, tiled=True)]
    dot_general x13 -> x0, matrix products: 23.7 us -> none  [the longest x5 11.4 us: add_products(): jnp.dot(normed, shard_rows, preferred_element_type=jnp.float32)]
    unnamed x59 -> x1, local copies, waits for them, and re-layouts: 16 us -> 1.67 us
    add x13 -> x0, other arithmetic: 12.6 us -> none  [the longest x5 9.41 us: gated_linear(): running = lax.associative_scan(combine, (jnp.exp(tail_decay), states))[1]]
  transfers between devices with their start and end apart: 8 -> 0, of which waited for: 6 -> 0; matrix products, arithmetic and copies ran while one was open for 21% -> 0% of each run, Pallas kernels for 0% -> 0%
where the time goes in v1:
time: 134 us; the launch traced here: 133 us
  Pallas kernels  132 us (99%)
  local copies, waits for them, and re-layouts  1.67 us (1%)
    pallas_call x1, Pallas kernels, on_device(): pl.pallas_call(functools.partial(layer_kernel, dims), out_shape=jax.Shape...  132 us

profile of v1, /device:TPU:33, one launch (start us, length us, event | category | flops | bytes accessed | tf_op | source)
XLA Modules:
  0.0 133.4 jit_solution(16919786146046909983)
XLA Ops:
  0.0 131.7 %layer.1 = bf16[512,256]{1,0:T(8,128)(2,1)} custom-call(bf16[512,256]{1,0:T(8,128)(2,1)} %x_hbm.1, bf16[128,128]{1,0:T(8,128)(2,1)} %q_hbm.1, bf16[128,128]{1,0:T(8,128)(2,1)} %k_hbm.1, bf16[128,256]{1,0:T(8,128)(2,1)} %v_hbm.1, bf16[256,128]{1,0:T(8,128)(2,1)} %comb_hbm.1, bf16[128,384]{1,0:T(8,128)(2,1)} %gate_hbm.1, bf16[128,384]{1,0:T(8,128)(2,1)} %up_hbm.1, ...), custom_call_target="tpu_custom_call" | custom-call | tf_op jit(solution)/shard_map/layer/pallas_call | solution.py:573
  131.7 1.7 %copy.21 = bf16[512,256]{1,0:T(8,128)(2,1)} copy(bf16[512,256]{1,0:T(8,128)(2,1)} %layer.1) | data formatting | bytes 524288

commit v2 on v1

v2 whole, which is shorter than its diff:
```python
import functools

import jax
import jax.numpy as jnp
from jax import lax
from jax.experimental import pallas as pl
from jax.experimental.pallas import tpu as pltpu
from jax.sharding import PartitionSpec as P

EPS = 1e-06
STEEPNESS = 16.0
MESH = pl.DeviceIdType.MESH
F32 = jnp.float32
BF16 = jnp.bfloat16
NEG = -1e30


def mm(a, b):
    return jnp.dot(a, b, preferred_element_type=F32)


def mm_nt(a, b):
    return lax.dot_general(a, b, (((1,), (1,)), ((), ())), preferred_element_type=F32)


def split2(v):
    hi = v.astype(BF16)
    return hi, (v - hi.astype(F32)).astype(BF16)


def layer_kernel(
    dims,
    x_hbm, q_hbm, k_hbm, v_hbm, comb_hbm, gate_hbm, up_hbm, down_hbm, exc_hbm,
    g1_ref, gaf_ref, gdi_ref, gdf_ref, egn_ref, left_ref, right_ref, const_ref, tapg_ref, tapu_ref,
    out_ref,
    back, xb, X, XG, F, wqkv, wc, wgu, wd, exc, ss, hout, hidden, G, firstb, acc, so, si, o2, orr, oll, ih, ifl,
    local_sem, zrecv, zsend, yrecv, ysend, agrecv, agsend, ssrecv, sssend, sibrecv, sibsend, rsrecv, rssend,
):
    NG, NZ, NTP = dims
    T, OC = xb.shape
    D = X.shape[1]
    NX = NTP // 2
    KD = q_hbm.shape[1]
    VD = v_hbm.shape[1]
    FU = gate_hbm.shape[1]
    RZ = q_hbm.shape[0]
    CZ = comb_hbm.shape[1]
    PER = OC // CZ
    H = T // 2
    HALF = NZ // 2

    g, z, t = lax.axis_index("grp"), lax.axis_index("fs"), lax.axis_index("tp")
    par = lax.rem(g, 2)
    pg = g + 1 - 2 * par
    xi, c = t // 2, lax.rem(t, 2)
    chip_r, chip_l, chip_2 = lax.rem(xi + 1, NX), lax.rem(xi + NX - 1, NX), lax.rem(xi + 2, NX)
    sib = 2 * xi + 1 - c
    tr, tl = 2 * chip_r + c, 2 * chip_l + c
    zr, zl = lax.rem(z + 1, NZ), lax.rem(z + NZ - 1, NZ)

    def m(v, n):
        return pl.multiple_of(v, n)

    def wview(ref, o, r0, rows):
        return ref.at[pl.ds(m(o * RZ + r0, 16), rows), :]

    def cview(ref, o, r0, rows):
        return ref.at[o // PER, pl.ds(m(r0, 16), rows), pl.ds(m(lax.rem(o, PER) * CZ, CZ), CZ)]

    def guview(o, r0, rows, c0, cols):
        return wgu.at[pl.ds(m(o * RZ + r0, 16), rows), pl.ds(m(c0, 128), cols)]

    VR = comb_hbm.shape[0]
    b_m, b_c = 80, VR - 160
    c_m = 2 * FU // 3
    d_m = FU // 3
    W = 2 * KD + VD
    PHASES = {
        "A": [(lambda o, p, i=i: wview(wqkv, o, p * 48 + 16 * i, 16), True, 16 * W) for i in range(3)]
        + [(lambda o, p, i=i: wview(wqkv, o, 96 + 16 * i, 16), False, 16 * W) for i in range((RZ - 96) // 16)],
        "B": [
            (lambda o, p: cview(wc, o, p * b_m, b_m), True, b_m * CZ),
            (lambda o, p: cview(wc, o, 2 * b_m, b_c), False, b_c * CZ),
        ],
        "P": [
            (lambda o, p: guview(o, 0, RZ // 2, p * c_m, c_m), True, RZ // 2 * c_m),
            (lambda o, p: guview(o, 0, RZ // 2, 2 * c_m, c_m), False, RZ // 2 * c_m),
        ],
        "Q": [
            (lambda o, p: guview(o, RZ // 2, RZ // 2, p * c_m, c_m), True, RZ // 2 * c_m),
            (lambda o, p: guview(o, RZ // 2, RZ // 2, 2 * c_m, c_m), False, RZ // 2 * c_m),
        ],
        "D": [
            (lambda o, p: cview(wd, o, p * d_m, d_m), True, d_m * CZ),
            (lambda o, p: cview(wd, o, 2 * d_m, d_m), False, d_m * CZ),
        ],
    }
    ANTIPODE = {"A": ((0, 2, 4), (1, 3)), "B": ((0,), (1,)), "P": ((0,), (1,)), "Q": ((1,), (0,)), "D": ((0,), (1,))}
    NAMES = list(PHASES)
    ZBASE, zn = {}, 0
    for name, chunks in PHASES.items():
        ZBASE[name] = zn
        zn += len(chunks)

    def block(elements):
        if elements % (16 * W) == 0:
            return wqkv.at[0 : elements // W, :]
        return wqkv.at[0 : elements // 128, 0:128]

    def arrived(sem, view):
        pltpu.make_async_remote_copy(
            src_ref=view, dst_ref=view, send_sem=sem, recv_sem=sem, device_id={"tp": sib}, device_id_type=MESH
        ).wait_recv()

    def left(sem, view):
        pltpu.make_async_remote_copy(
            src_ref=view, dst_ref=view, send_sem=sem, recv_sem=sem, device_id={"tp": sib}, device_id_type=MESH
        ).wait_send()

    sent_z = {(d, n): 0 for d in (0, 1) for n in NAMES}
    sent_y = {n: 0 for n in NAMES}

    def steps_from(d, s):
        return lax.rem(z + NZ - s, NZ) if d == 0 else lax.rem(z + s, NZ)

    def zstart(phase, ci, d, hop):
        view = PHASES[phase][ci][0](steps_from(d, hop), par)
        pltpu.make_async_remote_copy(
            src_ref=view, dst_ref=view,
            send_sem=zsend.at[d, NAMES.index(phase)], recv_sem=zrecv.at[ZBASE[phase] + ci, hop],
            device_id={"fs": zr if d == 0 else zl}, device_id_type=MESH,
        ).start()
        sent_z[d, phase] += PHASES[phase][ci][2]

    def ystart(phase, ci, d, s):
        view = PHASES[phase][ci][0](steps_from(d, s), par)
        i = NAMES.index(phase)
        pltpu.make_async_remote_copy(
            src_ref=view, dst_ref=view, send_sem=ysend.at[i], recv_sem=yrecv.at[i],
            device_id={"grp": pg}, device_id_type=MESH,
        ).start()
        sent_y[phase] += PHASES[phase][ci][2]

    def own_sends(phase):
        for ci in range(len(PHASES[phase])):
            for d in (0, 1):
                zstart(phase, ci, d, 0)

    deferred = []

    def y_flush():
        for args in deferred:
            ystart(*args)
        deferred.clear()

    def tick(phase, s, hold=False):
        for ci, (_, exchanged, elements) in enumerate(PHASES[phase]):
            dirs = [d for d in (0, 1) if s < HALF or ci in ANTIPODE[phase][d]]
            arrived(zrecv.at[ZBASE[phase] + ci, s - 1], block(elements * len(dirs)))
            for d in dirs:
                if s < HALF - 1 or (s == HALF - 1 and ci in ANTIPODE[phase][d]):
                    zstart(phase, ci, d, s)
            for d in dirs:
                if exchanged and hold:
                    deferred.append((phase, ci, d, s))
                elif exchanged:
                    ystart(phase, ci, d, s)

    def y_all(phase):
        arrived(yrecv.at[NAMES.index(phase)], block(sum(n for _, e, n in PHASES[phase] if e) * (NZ - 1)))

    zo = z
    locals_ = [
        (x_hbm, X.at[:, pl.ds(m(t * OC, OC), OC)]),
        (q_hbm, wqkv.at[pl.ds(m(zo * RZ, 16), RZ), 0:KD]),
        (k_hbm, wqkv.at[pl.ds(m(zo * RZ, 16), RZ), KD : 2 * KD]),
        (v_hbm, wqkv.at[pl.ds(m(zo * RZ, 16), RZ), 2 * KD : 2 * KD + VD]),
        (comb_hbm, cview(wc, zo, 0, VR)),
        (gate_hbm, wgu.at[pl.ds(m(zo * RZ, 16), RZ), 0:FU]),
        (up_hbm, wgu.at[pl.ds(m(zo * RZ, 16), RZ), FU : 2 * FU]),
        (down_hbm, cview(wd, zo, 0, FU)),
        (exc_hbm, exc),
        (x_hbm, xb),
    ]
    loads = [pltpu.make_async_copy(a, b, local_sem.at[i]) for i, (a, b) in enumerate(locals_)]
    for copy in loads:
        copy.start()

    back[...] = jnp.zeros_like(back)

    barrier = pltpu.get_barrier_semaphore()
    for d in range(1, NTP):
        pl.semaphore_signal(barrier, inc=1, device_id={"tp": lax.rem(t + d, NTP)}, device_id_type=MESH)
    for other in (zr, zl):
        pl.semaphore_signal(barrier, inc=1, device_id={"fs": other}, device_id_type=MESH)
    pl.semaphore_signal(barrier, inc=1, device_id={"grp": pg}, device_id_type=MESH)
    for i in range(0, 4):
        loads[i].wait()
    pl.semaphore_wait(barrier, NTP + 2)
    own_sends("A")

    row_iota = lax.broadcasted_iota(jnp.int32, (T, 1), 0)
    lane_iota = lax.broadcasted_iota(jnp.int32, (128, 128), 1)

    def gain_row(ref):
        per = OC // 128
        rows = [ref[pl.ds(t * per + i, 1), :] for i in range(per)]
        return jnp.concatenate(rows, axis=1)

    NB = T // 128

    def ss_store(k, cols):
        mat = jnp.zeros((128, 128), F32)
        for i, col in enumerate(cols):
            for j in range(NB):
                mat = jnp.where(lane_iota == i * NB + j, col[j * 128 : (j + 1) * 128], mat)
        ss[k, t] = mat.T[0:16, :]

    def settle(block_):
        rows = 16 if block_.dtype == BF16 else 8
        got = block_.reshape(-1, rows, block_.shape[-1])
        back[...] = back[...] + jnp.max(got, axis=0)[0:8, 0:128].astype(F32)

    def ss_start(k):
        settle(ss[k, t])
        for d in range(1, NTP):
            pltpu.make_async_remote_copy(
                src_ref=ss.at[k, t], dst_ref=ss.at[k, t], send_sem=sssend.at[k], recv_sem=ssrecv.at[k],
                device_id={"tp": lax.rem(t + d, NTP)}, device_id_type=MESH,
            ).start()

    def ss_total(k):
        arrived(ssrecv.at[k], ss.at[k, 0 : NTP - 1])
        total = ss[k, 0]
        for i in range(1, NTP):
            total = total + ss[k, i]
        return total

    def columns(rows):
        cols = jnp.concatenate([rows, jnp.zeros((120, 128), F32)], axis=0).T
        pick = lambda a: jnp.concatenate([cols[:, a + j : a + j + 1] for j in range(NB)], axis=0)
        return pick(0), pick(NB)

    def scale_into(scale, ref, lo, hi):
        for l in range(lo, hi):
            cols = slice(l * 128, (l + 1) * 128)
            XG[:, cols] = (X[:, cols].astype(F32) * scale * ref[l : l + 1, :]).astype(BF16)

    def part(buf, o, h):
        return buf.at[pl.ds(h * H, H), pl.ds(m(o * OC, OC), OC)]

    AG_SEM = (0, 1, 2, 3, 4, 5, 6, 6, 7, 8, 7, 8, 9, 9)

    def ag_send(buf, k, slot, o, h, dev):
        view = part(buf, o, h)
        pltpu.make_async_remote_copy(
            src_ref=view, dst_ref=view, send_sem=agsend.at[k], recv_sem=agrecv.at[k, AG_SEM[slot]],
            device_id={"tp": dev}, device_id_type=MESH,
        ).start()

    def ag_start(buf, k):
        for slot, h, dev in ((0, 0, tr), (2, 1, tl), (1, 1, tr), (3, 0, tl), (6, 0, sib), (7, 1, sib)):
            ag_send(buf, k, slot, t, h, dev)

    SRC = {0: (tl, 0), 1: (tl, 1), 2: (tr, 1), 3: (tr, 0), 4: (2 * chip_2 + c, 0), 5: (2 * chip_2 + c, 1)}

    def ag_take(buf, k, slots):
        for slot in slots:
            o, h = SRC[slot]
            arrived(agrecv.at[k, AG_SEM[slot]], part(buf, o, h))
            if slot == 0:
                ag_send(buf, k, 4, o, h, tr)
            if slot == 2:
                ag_send(buf, k, 5, o, h, tl)
            ag_send(buf, k, slot + 8, o, h, sib)

    SIB_SRC = {6: (sib, 0), 7: (sib, 1)}
    SIB_SRC.update({slot + 8: (o + 1 - 2 * c, h) for slot, (o, h) in SRC.items()})

    def ag_end(buf, k, pairs=((6, 7), (8, 10), (9, 11), (12, 13)), then=lambda o, h: None):
        for pair in pairs:
            arrived(agrecv.at[k, AG_SEM[pair[0]]], buf.at[:, 0:OC])
            for slot in pair:
                then(*SIB_SRC[slot])

    ag_start(X, 0)
    loads[9].wait()
    x32 = xb[...].astype(F32)
    ss_store(0, [jnp.sum(x32 * x32, axis=1, keepdims=True)])
    for i in range(4, 9):
        loads[i].wait()
    NL = D // 128

    tick("A", 1)
    ss_start(0)
    own_sends("B")
    tick("A", 2)
    ag_take(X, 0, (0, 2))
    tick("A", 3)
    ag_take(X, 0, (1, 3))
    tick("B", 1, True)
    tick("A", 4)
    tick("B", 2, True)
    ag_take(X, 0, (4, 5))
    tick("A", 5)
    tick("B", 3, True)
    ag_end(X, 0)
    total0 = ss_total(0)
    r1, _ = columns(lax.rsqrt(total0[0:8] / D + EPS))
    tick("A", 6)
    scale_into(r1, g1_ref, 0, NL // 2)
    tick("B", 4, True)
    tick("A", 7)
    scale_into(r1, g1_ref, NL // 2, NL)
    tick("B", 5, True)
    tick("A", 8)
    y_flush()
    tick("B", 6)
    y_all("A")
    own_sends("P")

    qk = mm(XG[...], wqkv[:, 0 : 2 * KD])
    q = qk[:, 0:KD].astype(BF16).astype(F32) * KD ** (-0.5)
    k = qk[:, KD : 2 * KD].astype(BF16).astype(F32)
    v = mm(XG[...], wqkv[:, 2 * KD : 2 * KD + VD]).astype(BF16)
    tick("B", 7)
    own_sends("Q")
    low = mm_nt(XG[...], left_ref[...])
    low_hi, low_lo = split2(low)
    right_hi, right_lo = split2(right_ref[...])
    pre = mm(low_hi, right_hi) + (mm(low_lo, right_hi) + mm(low_hi, right_lo)) + const_ref[...]
    ld = (jnp.minimum(pre, 0.0) - jnp.log1p(jnp.exp(-jnp.abs(pre)))) / STEEPNESS + exc[...]

    ri = lax.broadcasted_iota(jnp.int32, (128, 128), 0)
    tri = jnp.where(ri >= lane_iota, 1.0, 0.0).astype(BF16)
    ld_hi, ld_lo = split2(ld)
    pieces, carry = [], jnp.zeros((1, KD), F32)
    for j in range(T // 128):
        rows = slice(j * 128, (j + 1) * 128)
        run = mm(tri, ld_hi[rows]) + mm(tri, ld_lo[rows]) + carry
        carry = run[127:128]
        pieces.append(run)
    b = jnp.concatenate(pieces, axis=0)
    tick("B", 8)
    own_sends("D")

    def offsets(span):
        b3 = b.reshape(T // span, span, KD)
        return (b3 - b3[:, span // 2 - 1 : span // 2, :]).reshape(T, KD)

    def level(span):
        d = offsets(span)
        second = lax.rem(row_iota, span) >= span // 2
        e = jnp.exp(jnp.where(second, d, -d))
        return jnp.where(second, q * e, 0.0).astype(BF16), jnp.where(second, 0.0, k * e).astype(BF16)

    dd = offsets(32)
    qd_hi, qd_lo = split2(q * jnp.exp(dd))
    kd_hi, kd_lo = split2(k * jnp.exp(-dd))
    qd = jnp.concatenate([qd_hi, qd_lo, qd_hi], axis=1)
    kd = jnp.concatenate([kd_hi, kd_hi, kd_lo], axis=1)
    q64, k64 = level(64)
    q128, k128 = level(128)
    q256, k256 = level(256)
    q512, k512 = level(512)
    tick("P", 1)
    ci_ = lane_iota
    in32 = (ri // 32 == ci_ // 32) & (ri >= ci_)
    in64 = (ri // 64 == ci_ // 64) & (ri // 32 != ci_ // 32)
    diag = []
    for j in range(T // 128):
        rows = slice(j * 128, (j + 1) * 128)
        s = jnp.where(in32, mm_nt(qd[rows], kd[rows]), 0.0)
        s = s + jnp.where(in64, mm_nt(q64[rows], k64[rows]), 0.0)
        s = s + mm_nt(q128[rows], k128[rows])
        diag.append(s.astype(BF16))
    zero128 = jnp.zeros((128, 128), BF16)
    halves = []
    for j in range(2):
        lo = slice(j * 256, j * 256 + 128)
        hi = slice(j * 256 + 128, (j + 1) * 256)
        cross = mm_nt(q256[hi], k256[lo]).astype(BF16)
        top = mm(diag[2 * j], v[lo])
        bottom = mm(jnp.concatenate([cross, diag[2 * j + 1]], axis=1), v[j * 256 : (j + 1) * 256])
        halves.append(jnp.concatenate([top, bottom], axis=0))
    far = mm_nt(q512[256:512], k512[0:256]).astype(BF16)
    heads = jnp.concatenate([halves[0], halves[1] + mm(far, v[0:256])], axis=0)
    hs = lax.rsqrt(jnp.mean(heads * heads, axis=1, keepdims=True) + EPS)
    hout[...] = (heads * hs * egn_ref[...]).astype(BF16)
    tick("Q", 1)
    y_all("B")

    def rs(k, lhs_ref, w, between):
        order = (chip_2, chip_r, chip_l, xi)

        def products(n):
            so[k, n] = mm(lhs_ref[...], w[2 * order[n] + 1 - c]).astype(BF16)
            acc[n] = mm(lhs_ref[...], w[2 * order[n] + c])
            pltpu.make_async_remote_copy(
                src_ref=so.at[k, n], dst_ref=si.at[k, n], send_sem=sibsend.at[k], recv_sem=sibrecv.at[k, n],
                device_id={"tp": sib}, device_id_type=MESH,
            ).start()

        def send(sem, src, dst, dev):
            pltpu.make_async_remote_copy(
                src_ref=src, dst_ref=dst, send_sem=rssend.at[k], recv_sem=rsrecv.at[k, sem],
                device_id={"tp": dev}, device_id_type=MESH,
            ).start()

        def with_sib(n, rows):
            return acc[n, rows, :] + si[k, n, rows, :].astype(F32)

        lo, hi = pl.ds(0, H), pl.ds(H, H)
        products(0)
        products(1)
        between(0)
        arrived(sibrecv.at[k, 0], si.at[k, 0])
        o2[k, lo, :] = with_sib(0, lo).astype(BF16)
        o2[k, hi, :] = with_sib(0, hi).astype(BF16)
        settle(o2[k, hi, :])
        send(0, o2.at[k, lo], ih.at[k, 0], tr)
        send(1, o2.at[k, hi], ih.at[k, 1], tl)
        between(1)
        products(2)
        arrived(sibrecv.at[k, 1], si.at[k, 1])
        orr[k, hi, :] = with_sib(1, hi).astype(BF16)
        between(2)
        products(3)
        send(2, orr.at[k, hi], ifl.at[k, 0, hi], tr)
        arrived(sibrecv.at[k, 2], si.at[k, 2])
        oll[k, lo, :] = with_sib(2, lo).astype(BF16)
        acc[1, lo, :] = with_sib(1, lo)
        acc[2, hi, :] = with_sib(2, hi)
        settle(oll[k, lo, :])
        send(2, oll.at[k, lo], ifl.at[k, 1, lo], tl)
        between(3)
        arrived(rsrecv.at[k, 0], ih.at[k, 0])
        orr[k, lo, :] = (acc[1, lo, :] + ih[k, 0].astype(F32)).astype(BF16)
        arrived(rsrecv.at[k, 1], ih.at[k, 1])
        oll[k, hi, :] = (acc[2, hi, :] + ih[k, 1].astype(F32)).astype(BF16)
        settle(orr[k, lo, :])
        send(3, orr.at[k, lo], ifl.at[k, 0, lo], tr)
        arrived(sibrecv.at[k, 3], si.at[k, 3])
        settle(oll[k, hi, :])
        send(3, oll.at[k, hi], ifl.at[k, 1, hi], tl)
        acc[3] = acc[3] + si[k, 3].astype(F32)
        between(4)
        arrived(rsrecv.at[k, 2], ifl.at[k, 0])
        between(5)
        arrived(rsrecv.at[k, 3], ifl.at[k, 0])
        return acc[3] + (ifl[k, 0].astype(F32) + ifl[k, 1].astype(F32))

    WORK = (("P2",), ("Q2",), ("D1",), ("P3", "Q3"), ("D2", "P4", "Q4"), ("D3", "P5"))

    def ticks(*names):
        for name in names:
            tick(name[0], int(name[1]))

    def between0(i):
        ticks(*WORK[i])

    mixed = rs(0, hout, wc, between0)
    mg = mixed * gain_row(gaf_ref)
    F[:, pl.ds(m(t * OC, OC), OC)] = mg.astype(BF16)
    x32 = xb[...].astype(F32)
    ss_store(1, [jnp.sum(a, axis=1, keepdims=True) for a in (mixed * mixed, x32 * mg, mg * mg)])
    settle(F[H:T, pl.ds(m(t * OC, OC), OC)])
    ag_start(F, 1)
    acc[3] = mg
    ss_start(1)
    ticks("Q5", "D4", "P6")
    total1 = ss_total(1)
    ra_rows = lax.rsqrt(total1[0:NB] / D + EPS)
    squares = total0[0:NB] + 2.0 * ra_rows * total1[NB : 2 * NB] + ra_rows * ra_rows * total1[2 * NB : 3 * NB]
    ra, r2 = columns(jnp.concatenate([ra_rows, lax.rsqrt(squares / D + EPS)], axis=0))
    firstb[...] = (x32 + acc[3] * ra).astype(BF16)

    def join(o, h):
        rows, cols = pl.ds(h * H, H), pl.ds(m(o * OC, OC), OC)
        gain = jnp.concatenate([gdi_ref[pl.ds(o * (OC // 128) + i, 1), :] for i in range(OC // 128)], axis=1)
        whole = X[rows, cols].astype(F32) + F[rows, cols].astype(F32) * ra[h * H : (h + 1) * H]
        XG[rows, cols] = (whole * gain).astype(BF16)

    join(t, 0)
    join(t, 1)
    ticks("Q6", "D5")
    ag_take(F, 1, (0, 2))
    join(*SRC[0])
    join(*SRC[2])
    ag_end(F, 1, ((6, 7),), join)
    ticks("P7", "Q7", "D6")
    ag_take(F, 1, (1, 3))
    join(*SRC[1])
    join(*SRC[3])
    ag_end(F, 1, ((8, 10),), join)
    ticks("P8", "Q8", "D7")
    ag_take(F, 1, (4, 5))
    join(*SRC[4])
    join(*SRC[5])
    ag_end(F, 1, ((9, 11),), join)
    ticks("D8")
    y_all("P")
    y_all("Q")
    ag_end(F, 1, ((12, 13),), join)

    PAD = 8
    G[0:PAD, :] = jnp.zeros((PAD, 2 * FU), F32)
    for n in range(2 * FU // 256):
        cols = slice(n * 256, (n + 1) * 256)
        G[PAD : PAD + T, cols] = mm(XG[...], wgu[:, cols]) * r2

    def taps(ref, base):
        w = ref[:, base % FU : base % FU + 128].astype(F32)
        n = w.shape[0]
        total = None
        for j in range(n):
            term = w[j : j + 1] * G[PAD - (n - 1) + j : PAD - (n - 1) + j + T, base : base + 128]
            total = term if total is None else total + term
        return total

    for n in range(FU // 128):
        gc, uc = taps(tapg_ref, n * 128), taps(tapu_ref, FU + n * 128)
        hidden[:, n * 128 : (n + 1) * 128] = (gc / (1.0 + jnp.exp(-gc)) * uc).astype(BF16)
    y_all("D")
    channel = rs(1, hidden, wd, lambda i: None)
    ss_store(2, [jnp.sum(channel * channel, axis=1, keepdims=True)])
    acc[3] = channel
    ss_start(2)
    for i, name in enumerate(NAMES):
        for d in (0, 1):
            left(zsend.at[d, i], block(sent_z[d, name]))
        left(ysend.at[i], block(sent_y[name]))
    for k in (0, 1):
        left(agsend.at[k], X.at[0 : 14 * H * OC // D, :])
        left(sibsend.at[k], so.at[k])
        left(rssend.at[k], X.at[0 : 6 * H * OC // D, :])
        left(sssend.at[k], ss.at[k, 0 : NTP - 1])
    rc, _ = columns(lax.rsqrt(ss_total(2)[0:8] / D + EPS))
    out_ref[...] = (firstb[...].astype(F32) + acc[3] * rc * gain_row(gdf_ref)).astype(BF16)
    left(sssend.at[2], ss.at[2, 0 : NTP - 1])


def on_device(
    dims, x, g1, egn, gaf, gdi, gdf, wq, wk, wv, left, right, const, excess, comb, gate, up, tapg, tapu, down
):
    NG, NZ, NTP = dims
    T, OC = x.shape
    D = OC * NTP
    KD, VD, FU = wq.shape[1], wv.shape[1], gate.shape[1]
    any_ = pl.BlockSpec(memory_space=pl.ANY)
    vm = pl.BlockSpec(memory_space=pltpu.VMEM)
    DMA = pltpu.SemaphoreType.DMA
    NX = NTP // 2
    VM = pltpu.VMEM
    scratch = [
        VM((8, 128), F32), VM((T, OC), BF16), VM((T, D), BF16), VM((T, D), BF16), VM((T, D), BF16),
        VM((D, 2 * KD + VD), BF16), VM((NTP, comb.shape[0], OC), BF16), VM((D, 2 * FU), BF16), VM((NTP, FU, OC), BF16),
        VM((T, KD), F32), VM((3, NTP, 16, 128), F32),
        VM((T, VD), BF16), VM((T, FU), BF16), VM((T + 8, 2 * FU), F32), VM((T, OC), BF16),
        VM((NX, T, OC), F32), VM((2, NX, T, OC), BF16), VM((2, NX, T, OC), BF16),
        VM((2, T, OC), BF16), VM((2, T, OC), BF16), VM((2, T, OC), BF16),
        VM((2, 2, T // 2, OC), BF16), VM((2, 2, T, OC), BF16),
        DMA((10,)), DMA((13, NZ // 2)), DMA((2, 5)), DMA((5,)), DMA((5,)),
        DMA((2, 10)), DMA((2,)), DMA((3,)), DMA((3,)), DMA((2, NX)), DMA((2,)), DMA((2, 4)), DMA((2,)),
    ]
    return pl.pallas_call(
        functools.partial(layer_kernel, dims),
        out_shape=jax.ShapeDtypeStruct((T, OC), BF16),
        in_specs=[any_] * 9 + [vm] * 10,
        out_specs=vm,
        scratch_shapes=scratch,
        compiler_params=pltpu.CompilerParams(
            collective_id=0, has_side_effects=True, vmem_limit_bytes=60 * 1024 * 1024
        ),
        name="layer",
    )(
        x, wq, wk, wv, comb, gate, up, down, excess,
        g1.reshape(-1, 128), gaf.reshape(-1, 128), gdi.reshape(-1, 128), gdf.reshape(-1, 128),
        egn, left.T, right, const.reshape(1, -1), tapg, tapu,
    )


def solution(mesh):
    dims = (mesh.shape["grp"], mesh.shape["fs"], mesh.shape["tp"])
    placed = (
        P(("grp", "fs"), "tp"), P(), P("tp", None), P(), P(), P(), P("fs", "tp"), P("fs", "tp"), P("fs", "tp"), P(),
        P(None, "tp"), P("tp"), P(("grp", "fs"), "tp"), P("tp", "fs"), P("fs", "tp"), P("fs", "tp"), P(None, "tp"),
        P(None, "tp"), P("tp", "fs"),
    )
    return jax.shard_map(
        functools.partial(on_device, dims), mesh=mesh, in_specs=placed, out_specs=P(("grp", "fs"), "tp"),
        check_vma=False,
    )
```

time: 134 us -> 125 us (0.933)
  Pallas kernels: 132 us -> 123 us
    pallas_call x1, Pallas kernels: 132 us -> 123 us  [on_device(): pl.pallas_call(functools.partial(layer_kernel, dims), out_shape=jax.Shape...]
where the time goes in v2:
time: 125 us
  Pallas kernels  123 us (98%)
  local copies, waits for them, and re-layouts  1.67 us (1%)
    pallas_call x1, Pallas kernels, on_device(): pl.pallas_call(functools.partial(layer_kernel, dims), out_shape=jax.Shape...  123 us

profile of v2, /device:TPU:33, one launch (start us, length us, event | category | flops | bytes accessed | tf_op | source)
XLA Modules:
  0.0 124.8 jit_solution(17046520308697956268)
XLA Ops:
  0.0 123.1 %layer.1 = bf16[512,256]{1,0:T(8,128)(2,1)} custom-call(bf16[512,256]{1,0:T(8,128)(2,1)} %x_hbm.1, bf16[128,128]{1,0:T(8,128)(2,1)} %q_hbm.1, bf16[128,128]{1,0:T(8,128)(2,1)} %k_hbm.1, bf16[128,256]{1,0:T(8,128)(2,1)} %v_hbm.1, bf16[256,128]{1,0:T(8,128)(2,1)} %comb_hbm.1, bf16[128,384]{1,0:T(8,128)(2,1)} %gate_hbm.1, bf16[128,384]{1,0:T(8,128)(2,1)} %up_hbm.1, ...), custom_call_target="tpu_custom_call" | custom-call | tf_op jit(solution)/shard_map/layer/pallas_call | solution.py:566
  123.1 1.7 %copy.21 = bf16[512,256]{1,0:T(8,128)(2,1)} copy(bf16[512,256]{1,0:T(8,128)(2,1)} %layer.1) | data formatting | bytes 524288

commit v3 on v2

--- a/solution.py
+++ b/solution.py
@@ -342,6 +342,7 @@
         pieces.append(run)
     b = jnp.concatenate(pieces, axis=0)
     tick("B", 8)
+    tick("P", 1)
     own_sends("D")
 
     def offsets(span):
@@ -363,7 +364,7 @@
     q128, k128 = level(128)
     q256, k256 = level(256)
     q512, k512 = level(512)
-    tick("P", 1)
+    tick("Q", 1)
     ci_ = lane_iota
     in32 = (ri // 32 == ci_ // 32) & (ri >= ci_)
     in64 = (ri // 64 == ci_ // 64) & (ri // 32 != ci_ // 32)
@@ -387,7 +388,7 @@
     heads = jnp.concatenate([halves[0], halves[1] + mm(far, v[0:256])], axis=0)
     hs = lax.rsqrt(jnp.mean(heads * heads, axis=1, keepdims=True) + EPS)
     hout[...] = (heads * hs * egn_ref[...]).astype(BF16)
-    tick("Q", 1)
+    tick("P", 2)
     y_all("B")
 
     def rs(k, lhs_ref, w, between):
@@ -450,7 +451,7 @@
         arrived(rsrecv.at[k, 3], ifl.at[k, 0])
         return acc[3] + (ifl[k, 0].astype(F32) + ifl[k, 1].astype(F32))
 
-    WORK = (("P2",), ("Q2",), ("D1",), ("P3", "Q3"), ("D2", "P4", "Q4"), ("D3", "P5"))
+    WORK = (("Q2",), ("D1",), ("P3",), ("Q3", "P4"), ("D2", "Q4"), ("P5", "D3"))
 
     def ticks(*names):
         for name in names:
@@ -464,11 +465,13 @@
     F[:, pl.ds(m(t * OC, OC), OC)] = mg.astype(BF16)
     x32 = xb[...].astype(F32)
     ss_store(1, [jnp.sum(a, axis=1, keepdims=True) for a in (mixed * mixed, x32 * mg, mg * mg)])
+    ss_start(1)
     settle(F[H:T, pl.ds(m(t * OC, OC), OC)])
     ag_start(F, 1)
     acc[3] = mg
-    ss_start(1)
-    ticks("Q5", "D4", "P6")
+    ticks("Q5", "P6", "D4")
+    ag_take(F, 1, (0, 2))
+    ticks("Q6")
     total1 = ss_total(1)
     ra_rows = lax.rsqrt(total1[0:NB] / D + EPS)
     squares = total0[0:NB] + 2.0 * ra_rows * total1[NB : 2 * NB] + ra_rows * ra_rows * total1[2 * NB : 3 * NB]
@@ -483,31 +486,33 @@
 
     join(t, 0)
     join(t, 1)
-    ticks("Q6", "D5")
-    ag_take(F, 1, (0, 2))
     join(*SRC[0])
     join(*SRC[2])
     ag_end(F, 1, ((6, 7),), join)
-    ticks("P7", "Q7", "D6")
+    ticks("P7", "D5")
     ag_take(F, 1, (1, 3))
+    ticks("Q7")
     join(*SRC[1])
     join(*SRC[3])
     ag_end(F, 1, ((8, 10),), join)
-    ticks("P8", "Q8", "D7")
+    ticks("P8", "D6")
     ag_take(F, 1, (4, 5))
+    ticks("Q8")
     join(*SRC[4])
     join(*SRC[5])
     ag_end(F, 1, ((9, 11),), join)
-    ticks("D8")
+    ag_end(F, 1, ((12, 13),), join)
+    ticks("D7")
     y_all("P")
     y_all("Q")
-    ag_end(F, 1, ((12, 13),), join)
 
     PAD = 8
     G[0:PAD, :] = jnp.zeros((PAD, 2 * FU), F32)
     for n in range(2 * FU // 256):
         cols = slice(n * 256, (n + 1) * 256)
         G[PAD : PAD + T, cols] = mm(XG[...], wgu[:, cols]) * r2
+        if n == 1:
+            tick("D", 8)
 
     def taps(ref, base):
         w = ref[:, base % FU : base % FU + 128].astype(F32)

time: 125 us -> 124 us (level)
  no operation moved by 1% of the time
where the time goes in v3:
time: 124 us
  Pallas kernels  122 us (98%)
  local copies, waits for them, and re-layouts  1.67 us (1%)
    pallas_call x1, Pallas kernels, on_device(): pl.pallas_call(functools.partial(layer_kernel, dims), out_shape=jax.Shape...  122 us

profile of v3, /device:TPU:33, one launch (start us, length us, event | category | flops | bytes accessed | tf_op | source)
XLA Modules:
  0.0 123.6 jit_solution(7190487961021805309)
XLA Ops:
  0.0 121.9 %layer.1 = bf16[512,256]{1,0:T(8,128)(2,1)} custom-call(bf16[512,256]{1,0:T(8,128)(2,1)} %x_hbm.1, bf16[128,128]{1,0:T(8,128)(2,1)} %q_hbm.1, bf16[128,128]{1,0:T(8,128)(2,1)} %k_hbm.1, bf16[128,256]{1,0:T(8,128)(2,1)} %v_hbm.1, bf16[256,128]{1,0:T(8,128)(2,1)} %comb_hbm.1, bf16[128,384]{1,0:T(8,128)(2,1)} %gate_hbm.1, bf16[128,384]{1,0:T(8,128)(2,1)} %up_hbm.1, ...), custom_call_target="tpu_custom_call" | custom-call | tf_op jit(solution)/shard_map/layer/pallas_call | solution.py:571
  121.9 1.7 %copy.21 = bf16[512,256]{1,0:T(8,128)(2,1)} copy(bf16[512,256]{1,0:T(8,128)(2,1)} %layer.1) | data formatting | bytes 524288

commit v4 on v3

--- a/solution.py
+++ b/solution.py
@@ -67,13 +67,9 @@
     def cview(ref, o, r0, rows):
         return ref.at[o // PER, pl.ds(m(r0, 16), rows), pl.ds(m(lax.rem(o, PER) * CZ, CZ), CZ)]
 
-    def guview(o, r0, rows, c0, cols):
-        return wgu.at[pl.ds(m(o * RZ + r0, 16), rows), pl.ds(m(c0, 128), cols)]
-
     VR = comb_hbm.shape[0]
-    b_m, b_c = 80, VR - 160
-    c_m = 2 * FU // 3
-    d_m = FU // 3
+    b_m, b_c = 96, VR - 192
+    d_m, d_c = 144, FU - 288
     W = 2 * KD + VD
     PHASES = {
         "A": [(lambda o, p, i=i: wview(wqkv, o, p * 48 + 16 * i, 16), True, 16 * W) for i in range(3)]
@@ -82,20 +78,14 @@
             (lambda o, p: cview(wc, o, p * b_m, b_m), True, b_m * CZ),
             (lambda o, p: cview(wc, o, 2 * b_m, b_c), False, b_c * CZ),
         ],
-        "P": [
-            (lambda o, p: guview(o, 0, RZ // 2, p * c_m, c_m), True, RZ // 2 * c_m),
-            (lambda o, p: guview(o, 0, RZ // 2, 2 * c_m, c_m), False, RZ // 2 * c_m),
-        ],
-        "Q": [
-            (lambda o, p: guview(o, RZ // 2, RZ // 2, p * c_m, c_m), True, RZ // 2 * c_m),
-            (lambda o, p: guview(o, RZ // 2, RZ // 2, 2 * c_m, c_m), False, RZ // 2 * c_m),
-        ],
+        "P": [(lambda o, p, i=i: wview(wgu, o, p * 48 + 16 * i, 16), True, 16 * 2 * FU) for i in range(3)],
+        "Q": [(lambda o, p, i=i: wview(wgu, o, 96 + 16 * i, 16), False, 16 * 2 * FU) for i in range((RZ - 96) // 16)],
         "D": [
             (lambda o, p: cview(wd, o, p * d_m, d_m), True, d_m * CZ),
-            (lambda o, p: cview(wd, o, 2 * d_m, d_m), False, d_m * CZ),
+            (lambda o, p: cview(wd, o, 2 * d_m, d_c), False, d_c * CZ),
         ],
     }
-    ANTIPODE = {"A": ((0, 2, 4), (1, 3)), "B": ((0,), (1,)), "P": ((0,), (1,)), "Q": ((1,), (0,)), "D": ((0,), (1,))}
+    ANTIPODE = {"A": ((0, 2, 4), (1, 3)), "B": ((0,), (1,)), "P": ((0,), (1, 2)), "Q": ((0,), (1,)), "D": ((0,), (1,))}
     NAMES = list(PHASES)
     ZBASE, zn = {}, 0
     for name, chunks in PHASES.items():
@@ -103,9 +93,11 @@
         zn += len(chunks)
 
     def block(elements):
-        if elements % (16 * W) == 0:
-            return wqkv.at[0 : elements // W, :]
-        return wqkv.at[0 : elements // 128, 0:128]
+        for ref, wide in ((wgu, 2 * FU), (wqkv, W), (wgu, FU), (wqkv, 128)):
+            rows = elements // wide
+            if elements % (16 * wide) == 0 and rows <= D:
+                return ref.at[0:rows, 0:wide]
+        raise ValueError(elements)
 
     def arrived(sem, view):
         pltpu.make_async_remote_copy(
@@ -504,7 +496,6 @@
     ag_end(F, 1, ((12, 13),), join)
     ticks("D7")
     y_all("P")
-    y_all("Q")
 
     PAD = 8
     G[0:PAD, :] = jnp.zeros((PAD, 2 * FU), F32)
@@ -534,7 +525,8 @@
     for i, name in enumerate(NAMES):
         for d in (0, 1):
             left(zsend.at[d, i], block(sent_z[d, name]))
-        left(ysend.at[i], block(sent_y[name]))
+        if sent_y[name]:
+            left(ysend.at[i], block(sent_y[name]))
     for k in (0, 1):
         left(agsend.at[k], X.at[0 : 14 * H * OC // D, :])
         left(sibsend.at[k], so.at[k])
@@ -565,7 +557,7 @@
         VM((NX, T, OC), F32), VM((2, NX, T, OC), BF16), VM((2, NX, T, OC), BF16),
         VM((2, T, OC), BF16), VM((2, T, OC), BF16), VM((2, T, OC), BF16),
         VM((2, 2, T // 2, OC), BF16), VM((2, 2, T, OC), BF16),
-        DMA((10,)), DMA((13, NZ // 2)), DMA((2, 5)), DMA((5,)), DMA((5,)),
+        DMA((10,)), DMA((14, NZ // 2)), DMA((2, 5)), DMA((5,)), DMA((5,)),
         DMA((2, 10)), DMA((2,)), DMA((3,)), DMA((3,)), DMA((2, NX)), DMA((2,)), DMA((2, 4)), DMA((2,)),
     ]
     return pl.pallas_call(

time: 124 us -> 123 us (level)
  no operation moved by 1% of the time
where the time goes in v4:
time: 123 us
  Pallas kernels  121 us (98%)
  local copies, waits for them, and re-layouts  1.67 us (1%)
    pallas_call x1, Pallas kernels, on_device(): pl.pallas_call(functools.partial(layer_kernel, dims), out_shape=jax.Shape...  121 us

profile of v4, /device:TPU:33, one launch (start us, length us, event | category | flops | bytes accessed | tf_op | source)
XLA Modules:
  0.0 122.8 jit_solution(10474891601376719975)
XLA Ops:
  0.0 121.1 %layer.1 = bf16[512,256]{1,0:T(8,128)(2,1)} custom-call(bf16[512,256]{1,0:T(8,128)(2,1)} %x_hbm.1, bf16[128,128]{1,0:T(8,128)(2,1)} %q_hbm.1, bf16[128,128]{1,0:T(8,128)(2,1)} %k_hbm.1, bf16[128,256]{1,0:T(8,128)(2,1)} %v_hbm.1, bf16[256,128]{1,0:T(8,128)(2,1)} %comb_hbm.1, bf16[128,384]{1,0:T(8,128)(2,1)} %gate_hbm.1, bf16[128,384]{1,0:T(8,128)(2,1)} %up_hbm.1, ...), custom_call_target="tpu_custom_call" | custom-call | tf_op jit(solution)/shard_map/layer/pallas_call | solution.py:563
  121.1 1.7 %copy.21 = bf16[512,256]{1,0:T(8,128)(2,1)} copy(bf16[512,256]{1,0:T(8,128)(2,1)} %layer.1) | data formatting | bytes 524288

commit v5 on v4

--- a/solution.py
+++ b/solution.py
@@ -287,27 +287,28 @@
     ss_start(0)
     own_sends("B")
     tick("A", 2)
+    tick("B", 1, True)
     ag_take(X, 0, (0, 2))
     tick("A", 3)
+    tick("B", 2, True)
     ag_take(X, 0, (1, 3))
-    tick("B", 1, True)
     tick("A", 4)
-    tick("B", 2, True)
+    tick("B", 3, True)
     ag_take(X, 0, (4, 5))
     tick("A", 5)
-    tick("B", 3, True)
+    tick("B", 4, True)
     ag_end(X, 0)
     total0 = ss_total(0)
     r1, _ = columns(lax.rsqrt(total0[0:8] / D + EPS))
     tick("A", 6)
     scale_into(r1, g1_ref, 0, NL // 2)
-    tick("B", 4, True)
+    tick("B", 5, True)
     tick("A", 7)
     scale_into(r1, g1_ref, NL // 2, NL)
-    tick("B", 5, True)
+    tick("B", 6, True)
     tick("A", 8)
     y_flush()
-    tick("B", 6)
+    tick("B", 7)
     y_all("A")
     own_sends("P")
 
@@ -315,7 +316,7 @@
     q = qk[:, 0:KD].astype(BF16).astype(F32) * KD ** (-0.5)
     k = qk[:, KD : 2 * KD].astype(BF16).astype(F32)
     v = mm(XG[...], wqkv[:, 2 * KD : 2 * KD + VD]).astype(BF16)
-    tick("B", 7)
+    tick("B", 8)
     own_sends("Q")
     low = mm_nt(XG[...], left_ref[...])
     low_hi, low_lo = split2(low)
@@ -333,7 +334,6 @@
         carry = run[127:128]
         pieces.append(run)
     b = jnp.concatenate(pieces, axis=0)
-    tick("B", 8)
     tick("P", 1)
     own_sends("D")
 

time: 123 us -> 122 us (level)
  no operation moved by 1% of the time
where the time goes in v5:
time: 122 us
  Pallas kernels  120 us (98%)
  local copies, waits for them, and re-layouts  1.67 us (1%)
    pallas_call x1, Pallas kernels, on_device(): pl.pallas_call(functools.partial(layer_kernel, dims), out_shape=jax.Shape...  120 us

profile of v5, /device:TPU:33, one launch (start us, length us, event | category | flops | bytes accessed | tf_op | source)
XLA Modules:
  0.0 121.7 jit_solution(10311125713558391358)
XLA Ops:
  0.0 120.1 %layer.1 = bf16[512,256]{1,0:T(8,128)(2,1)} custom-call(bf16[512,256]{1,0:T(8,128)(2,1)} %x_hbm.1, bf16[128,128]{1,0:T(8,128)(2,1)} %q_hbm.1, bf16[128,128]{1,0:T(8,128)(2,1)} %k_hbm.1, bf16[128,256]{1,0:T(8,128)(2,1)} %v_hbm.1, bf16[256,128]{1,0:T(8,128)(2,1)} %comb_hbm.1, bf16[128,384]{1,0:T(8,128)(2,1)} %gate_hbm.1, bf16[128,384]{1,0:T(8,128)(2,1)} %up_hbm.1, ...), custom_call_target="tpu_custom_call" | custom-call | tf_op jit(solution)/shard_map/layer/pallas_call | solution.py:563
  120.1 1.7 %copy.21 = bf16[512,256]{1,0:T(8,128)(2,1)} copy(bf16[512,256]{1,0:T(8,128)(2,1)} %layer.1) | data formatting | bytes 524288
